TPU v7x, 128 devices: a whole 4x4x4 slice. The times are simulated.
128 devices in a mesh: sp: 16 (over z, y), tp: 8 (over x, core).
Axes of the slice: x: 4, y: 4, z: 4, core: 2. Of those that a mesh axis runs over, the one named last changes fastest.
Arguments:
- inputs: bfloat16 [8192, 4096], P(('sp', 'tp')), may hold values from -42 to 42
- a_query_w: bfloat16 [4096, 2048], P(None, 'tp'), may hold values from -0.12570312 to 0.12570312
- a_key_w: bfloat16 [4096, 2048], P(None, 'tp'), may hold values from -0.12570312 to 0.12570312
- a_value_w: bfloat16 [4096, 2048], P(None, 'tp'), may hold values from -0.09375 to 0.09375
- b_query_w: bfloat16 [4096, 2048], P(None, 'tp'), may hold values from -0.12570312 to 0.12570312
- b_key_w: bfloat16 [4096, 512], P(None, 'tp'), may hold values from -0.12570312 to 0.12570312
- b_value_w: bfloat16 [4096, 512], P(None, 'tp'), may hold values from -0.09375 to 0.09375
- head_lambda: float32 [16], P('tp'), may hold values from 0.3 to 0.8
- head_gain: float32 [128], replicated, may hold values from 0.1 to 1.9
- sink_logit: float32 [32], P('tp'), may hold values from 2 to 7
- a_out_w: bfloat16 [2048, 4096], P('tp'), may hold values from -0.125 to 0.125
- b_out_w: bfloat16 [2048, 4096], P('tp'), may hold values from -0.625 to 0.625
Outputs:
- mixed: bfloat16 [8192, 4096], P(('sp', 'tp'))
All inputs are finite; a program needn't handle non-finite values.
Results may differ from a plain program's by a relative error of at most 0.015.
Values may be sent and summed in bfloat16 or wider, within the bound.
A program may use at most 128 MiB of HBM per device.

v0:
```python
import math

import jax
import jax.numpy as jnp
from jax import lax
from jax.sharding import PartitionSpec as P

HEAD_DIM = 64
VALUE_DIM = 128
WINDOW = 128


norm_eps = 0.0001
head_scale = 0.8
mask_fill = -1e30


def from_behind(value, axis, by):
    size = lax.axis_size(axis)
    pairs = [(i, i + by) for i in range(size) if 0 <= i + by < size]
    return lax.ppermute(value, axis, pairs)


def side_by_side(arrays, axis, dim, along):
    widths = [a.shape[along] for a in arrays]
    both = jnp.concatenate(arrays, axis=along)
    whole = lax.all_gather(both, axis, axis=dim, tiled=True)
    return tuple(jnp.split(whole, [sum(widths[:k]) for k in range(1, len(widths))], axis=along))


def key_span(row_count):
    span_rows = math.gcd(row_count, 1024)
    return span_rows


def attend_block(carried, queries, query_pos, block_keys, block_values, key_pos):
    running, totals, numerator = carried
    scores = jnp.einsum(
        "qhmd,khmd->hmqk", queries, block_keys, preferred_element_type=jnp.float32
    ) * HEAD_DIM ** (-0.5)
    allowed = query_pos[:, None] >= key_pos[None, :]
    scores = jnp.where(allowed, scores, mask_fill)
    updated = jnp.maximum(running, jnp.max(scores, axis=-1))
    weights = jnp.where(allowed, jnp.exp(scores - updated[..., None]), 0.0)
    shrink = jnp.exp(running - updated)
    totals = totals * shrink + jnp.sum(weights, axis=-1)
    numerator = numerator * shrink[..., None] + jnp.einsum(
        "hmqk,khe->hmqe",
        weights.astype(jnp.bfloat16),
        block_values,
        preferred_element_type=jnp.float32,
    )
    return (updated, totals, numerator)


def advance(states, groups, key_rows, value_rows):
    row_count = key_rows.shape[0]
    span_rows = key_span(row_count)
    local_heads = value_rows.shape[1] // VALUE_DIM
    key_rows = key_rows.reshape(row_count, local_heads, 2, HEAD_DIM)
    value_rows = value_rows.reshape(row_count, local_heads, VALUE_DIM)

    def one_span(span_index, current):
        span_start = span_index * span_rows
        block_keys = lax.dynamic_slice_in_dim(key_rows, span_start, span_rows, 0)
        block_values = lax.dynamic_slice_in_dim(value_rows, span_start, span_rows, 0)
        key_pos = span_start + jnp.arange(span_rows, dtype=jnp.int32)
        results = []
        for query_group, carried in zip(groups, current):
            queries, query_pos = query_group

            def compute(given_state, queries=queries, query_pos=query_pos):
                return attend_block(
                    given_state, queries, query_pos, block_keys, block_values, key_pos
                )

            def unchanged(given_state):
                return given_state

            results.append(lax.cond(key_pos[0] <= query_pos[-1], compute, unchanged, carried))
        return tuple(results)

    return lax.fori_loop(0, row_count // span_rows, one_span, states)


def finish_heads(carried, head_lambda, head_gain):
    running, totals, numerator = carried
    means = numerator / totals[..., None]
    difference = means[:, 0] - head_lambda[:, None, None] * means[:, 1]
    mean_square = jnp.mean(difference * difference, axis=-1, keepdims=True)
    return (difference * lax.rsqrt(mean_square + norm_eps) * head_gain * head_scale).astype(
        jnp.bfloat16
    )


def shards(
    inputs,
    a_query_w,
    a_key_w,
    a_value_w,
    b_query_w,
    b_key_w,
    b_value_w,
    head_lambda,
    head_gain,
    sink_logit,
    a_out_w,
    b_out_w,
):
    matrices = (a_query_w, a_key_w, a_value_w, b_query_w, b_key_w, b_value_w)

    def project(shard_piece):
        return jnp.concatenate(
            [
                jnp.dot(shard_piece, matrix, preferred_element_type=jnp.float32).astype(
                    jnp.bfloat16
                )
                for matrix in matrices
            ],
            axis=1,
        )

    projected = project(lax.all_gather(inputs, "tp", axis=0, tiled=True))
    seg_rows = projected.shape[0]
    column_edges = [0]
    for matrix in matrices:
        column_edges.append(column_edges[-1] + matrix.shape[1])
    a_query = projected[:, column_edges[0] : column_edges[1]]
    a_key = projected[:, column_edges[1] : column_edges[2]]
    a_value = projected[:, column_edges[2] : column_edges[3]]
    b_query = projected[:, column_edges[3] : column_edges[4]]
    b_pair = projected[:, column_edges[4] : column_edges[6]]
    local_heads = head_lambda.shape[0]
    offset = lax.axis_index("sp") * seg_rows
    positions = offset + jnp.arange(seg_rows, dtype=jnp.int32)
    query_heads = a_query.reshape(seg_rows, local_heads, 2, HEAD_DIM)
    groups = ((query_heads, positions),)
    initial = tuple(
        (
            (
                jnp.full((local_heads, 2, group_queries.shape[0]), mask_fill, jnp.float32),
                jnp.zeros((local_heads, 2, group_queries.shape[0]), jnp.float32),
                jnp.zeros((local_heads, 2, group_queries.shape[0], VALUE_DIM), jnp.float32),
            )
            for group_queries, group_pos in groups
        )
    )
    earlier = from_behind(b_pair[seg_rows - WINDOW :], "sp", 1)
    shard_piece = side_by_side((a_key, a_value), "sp", 0, 1)
    states = advance(initial, groups, shard_piece[0], shard_piece[1])
    finished = [finish_heads(carried, head_lambda, head_gain) for carried in states]
    a_heads = finished[0]
    kv_heads = b_pair.shape[1] // (2 * HEAD_DIM)
    group_size = b_query.shape[1] // HEAD_DIM // kv_heads
    extended = jnp.concatenate([earlier, b_pair], axis=0)
    near_keys = extended[:, : kv_heads * HEAD_DIM].reshape(WINDOW + seg_rows, kv_heads, HEAD_DIM)
    near_values = extended[:, kv_heads * HEAD_DIM :].reshape(WINDOW + seg_rows, kv_heads, HEAD_DIM)
    window_queries = b_query.reshape(seg_rows, kv_heads, group_size, HEAD_DIM)
    sink_term = sink_logit.reshape(kv_heads, group_size)[:, :, None]
    query_span = math.gcd(seg_rows, 512)
    scores = jnp.einsum(
        "qhgd,khd->hgqk", window_queries, near_keys, preferred_element_type=jnp.float32
    ) * HEAD_DIM ** (-0.5)
    query_pos = offset + 0 + jnp.arange(query_span, dtype=jnp.int32)
    near_pos = offset + 0 - WINDOW + jnp.arange(query_span + WINDOW, dtype=jnp.int32)
    distance = query_pos[:, None] - near_pos[None, :]
    allowed = (distance >= 0) & (distance < WINDOW) & (near_pos[None, :] >= 0)
    scores = jnp.where(allowed, scores, mask_fill)
    row_top = jnp.maximum(jnp.max(scores, axis=-1), sink_term)
    weights = jnp.where(allowed, jnp.exp(scores - row_top[..., None]), 0.0)
    row_total = jnp.sum(weights, axis=-1) + jnp.exp(sink_term - row_top)
    probs = (weights / row_total[..., None]).astype(jnp.bfloat16)
    block_out = jnp.einsum("hgqk,khd->qhgd", probs, near_values, preferred_element_type=jnp.float32)
    outputs = block_out.astype(jnp.bfloat16).reshape(query_span, kv_heads * group_size * HEAD_DIM)
    a_weight = a_out_w.reshape(local_heads, VALUE_DIM, a_out_w.shape[1])
    return lax.psum_scatter(
        (
            jnp.einsum("hqe,hen->qn", a_heads, a_weight, preferred_element_type=jnp.float32)
            + jnp.dot(outputs, b_out_w, preferred_element_type=jnp.float32)
        ).astype(jnp.bfloat16),
        "tp",
        scatter_dimension=0,
        tiled=True,
    )


def solution(mesh):
    return jax.shard_map(
        shards,
        mesh=mesh,
        in_specs=(
            P(("sp", "tp"), None),
            P(None, "tp"),
            P(None, "tp"),
            P(None, "tp"),
            P(None, "tp"),
            P(None, "tp"),
            P(None, "tp"),
            P("tp"),
            P(),
            P("tp"),
            P("tp", None),
            P("tp", None),
        ),
        out_specs=P(("sp", "tp"), None),
        check_vma=False,
    )
```

profile of v0, /device:TPU:1, one launch (start us, length us, event | category | flops | bytes accessed | tf_op | source)
XLA Modules:
  0.0 286.6 jit_solution(3257539258130049300)
XLA Ops:
  6.5 0.7 all-gather.3.cloned.1.call-update
  7.3 37.4 %all-gather.3.cloned.1.call-done = bf16[512,4096]{1,0:T(8,128)(2,1)} async-done(((bf16[64,4096]{1,0:T(8,128)(2,1)}), bf16[512,4096]{1,0:T(8,128)(2,1)}) %all-gather.3.cloned.1.call-update) | async-done | bytes 4194320 | tf_op jit(solution)/shard_map/all_gather | solution.py:123
  44.7 4.3 %convolution_convert_fusion.2 = bf16[512,256]{0,1:T(8,128)(2,1)S(1)} fusion(bf16[512,4096]{1,0:T(8,128)(2,1)} %all-gather.3.cloned.1.call-done, bf16[4096,256]{1,0:T(8,128)(2,1)} %param.19), kind=kOutput, calls=%fused_computation.37 | convolution fusion | flops 1073872896 | bytes 6553600 | tf_op jit(solution)/shard_map/dot_general | solution.py:115
  49.4 1.3 convolution_convert_fusion.3
  50.7 0.8 pad_maximum_fusion
  52.1 3.8 %convolution_convert_fusion.4 = bf16[512,64]{0,1:T(8,128)(2,1)S(1)} fusion(bf16[512,4096]{1,0:T(8,128)(2,1)} %all-gather.3.cloned.1.call-done, bf16[4096,64]{0,1:T(8,128)(2,1)S(1)} %copy-done.4), kind=kOutput, calls=%fused_computation.39 | convolution fusion | flops 268468224 | bytes 4784128 | tf_op jit(solution)/shard_map/dot_general | solution.py:115
  56.0 1.4 convolution_convert_fusion.5
  57.4 3.2 %collective-permute-start = (bf16[128,128]{0,1:T(8,128)(2,1)S(1)}, bf16[128,128]{0,1:T(8,128)(2,1)S(1)}, u32[]{:S(2)}, u32[]{:S(2)}) collective-permute-start(bf16[128,128]{0,1:T(8,128)(2,1)S(1)} %pad_maximum_fusion.1), channel_id=1, source_target_pairs={{0,8},{8,16},{16,24},{24,32},{32,40},{40,48},{48,56},{56,64},{64,7... | collective-permute-start | bytes 98312 | tf_op jit(solution)/shard_map/ppermute | solution.py:21
  60.7 1.3 convolution_convert_fusion
  62.0 2.0 convolution_convert_fusion.1
  64.0 1.1 fusion.19
  65.2 1.3 fusion.20
  66.5 1.8 fusion.25
  68.4 59.0 %all-gather.5.cloned.1.call-done = bf16[8192,512]{0,1:T(8,128)(2,1)} async-done(((bf16[512,512]{0,1:T(8,128)(2,1)}), bf16[8192,512]{0,1:T(8,128)(2,1)}) %all-gather.5.cloned.1.call-update) | async-done | bytes 8388624 | tf_op jit(solution)/shard_map/all_gather | solution.py:27
  127.3 5.9 %fusion.40 = (bf16[8192,256]{0,1:T(8,128)(2,1)}, bf16[8192,256]{0,1:T(8,128)(2,1)}) fusion(bf16[8192,512]{0,1:T(8,128)(2,1)} %all-gather.5.cloned.1.call-done), kind=kLoop, calls=%fused_computation.68 | loop fusion | bytes 16777216 | tf_op jit(solution)/shard_map/split | solution.py:28
  133.2 6.3 %copy.14 = bf16[8192,2,128]{2,0,1:T(8,128)(2,1)} copy(bf16[8192,2,128]{0,2,1:T(8,128)(2,1)} %bitcast.105) | data formatting | bytes 8388608 | tf_op jit(solution)/shard_map/while | solution.py:83
  139.6 31.0 %while.17 = (s32[]{:T(128)}, f32[2,2,512]{2,1,0:T(2,128)S(1)}, f32[2,2,512]{2,1,0:T(2,128)S(1)}, f32[2,2,512,128]{3,2,1,0:T(8,128)S(1)}, s32[512]{0:T(512)S(1)},...) while((s32[]{:T(128)}, f32[2,2,512]{2,1,0:T(2,128)S(1)}, ...), condition=%wide.region_5.6_spmd, body=%wide.region_0.5_spmd.sunk | while | flops 833623040 | bytes 30812476 | solution.py:83
  139.7 0.6 slice.65
  142.3 9.8 %conditional.2 = ((f32[2,2,512]{2,1,0:T(2,128)S(1)}, f32[2,2,512]{2,1,0:T(2,128)S(1)}, f32[2,2,512,128]{3,2,1,0:T(8,128)S(1)})) conditional(s32[]{:T(128)} %bitcast.103, (f32[2,2,512]{2,1,0:T(2,128)S(1)}, f32[2,2,512]{2,1,0:T(2,128)S(1)}, f32[2,2,512,128]{3,2,1,0:T(8,128)S(1)}) %tuple.51, (s32[512]{0:T(512)S(1)}, s32[1024]{0:T(1024)S(1)}, s32[]{:T(128)}, ...), branch_computations={%region_1.0_spmd, %region_2.4_spmd} | conditional | flops 833622016 | bytes 30808138 | solution.py:80
  142.7 2.7 fusion
  145.4 2.1 fusion.2
  147.5 4.5 %fusion.6 = f32[2,2,512,128]{3,2,1,0:T(8,128)S(1)} fusion(f32[2,2,1024,512]{3,2,1,0:T(8,128)S(1)} %get-tuple-element.290, f32[2,2,512]{2,1,0:T(2,128)S(1)} %max.21, pred[512,1024]{0,1:T(8,128)(4,1)S(1)} %broadcast_compare_fusion, f32[2,2,512,128]{3,2,1,0:T(8,128)S(1)} %get-tuple-element.245, bf16[8192,2,128]{2,0,1:T(8,128)(2,1)} %get-tuple-element.246, ...), kind=kOutput, calls=%fused_computation.7 | convolution fusion | flops 547880960 | bytes 11550724 | tf_op jit(solution)/shard_map/while/body/eval_jaxpr/cond/branch_1_fun/hmqk,khe->hmqe/dot_general | solution.py:47
  152.1 0.6 slice.65
  154.7 0.6 slice.65
  157.4 0.6 slice.65
  160.1 0.6 slice.65
  162.7 0.6 slice.65
  165.4 0.6 slice.65
  168.0 0.6 slice.65
  171.4 1.3 fusion.30
  173.0 3.3 %fusion.18 = bf16[512,4096]{1,0:T(8,128)(2,1)} fusion(f32[512,4096,1]{1,0,2:T(8,128)S(1)} %fusion.30, bf16[512,256]{0,1:T(8,128)(2,1)S(1)} %bitcast.107, bf16[256,4096]{1,0:T(8,128)(2,1)S(1)} %copy-done.3), kind=kOutput, calls=%fused_computation.22 | convolution fusion | flops 1077936128 | bytes 14942208 | tf_op jit(solution)/shard_map/dot_general | solution.py:179
  176.2 103.8 %reduce-scatter.2.cloned.1.call-done = bf16[64,4096]{1,0:T(8,128)(2,1)} async-done(((bf16[512,4096]{1,0:T(8,128)(2,1)}), bf16[64,4096]{1,0:T(8,128)(2,1)}) %reduce-scatter.2.cloned.1.call-update) | async-done | bytes 524304 | tf_op jit(solution)/shard_map/reduce_scatter | solution.py:176
  (71 shorter events, 7.4 us)
Async XLA Ops:
  6.5 164.8 %copy-start = (bf16[256,4096]{1,0:T(8,128)(2,1)S(1)}, bf16[256,4096]{1,0:T(8,128)(2,1)}, u32[]{:S(2)}) copy-start(bf16[256,4096]{1,0:T(8,128)(2,1)} %param.26) | copy-start | bytes 6291460
  6.5 38.2 %all-gather.3.cloned.1.call-start = ((), (), s32[]{:S(2)}) async-start(), calls=%async_computation.1 | async-start | bytes 4718592 | tf_op jit(solution)/shard_map/all_gather | solution.py:123
  7.3 120.1 %all-gather.5.cloned.1.call-start = ((), (), s32[]{:S(2)}) async-start(), calls=%async_computation.2 | async-start | bytes 8912896 | tf_op jit(solution)/shard_map/all_gather | solution.py:27
  44.7 4.3 %copy-start.1 = (bf16[512,4096]{1,0:T(8,128)(2,1)S(1)}, bf16[512,4096]{1,0:T(8,128)(2,1)}, u32[]{:S(2)}) copy-start(bf16[512,4096]{1,0:T(8,128)(2,1)} %all-gather.3.cloned.1.call-done) | copy-start | bytes 12582916
  44.7 4.7 %copy-start.9 = (bf16[4096,256]{1,0:T(8,128)(2,1)S(1)}, bf16[4096,256]{1,0:T(8,128)(2,1)}, u32[]{:S(2)}) copy-start(bf16[4096,256]{1,0:T(8,128)(2,1)} %param.18) | copy-start | bytes 6291460
  49.4 2.7 copy-start.4
  50.7 5.2 %copy-start.5 = (bf16[4096,64]{0,1:T(8,128)(2,1)S(1)}, bf16[4096,64]{0,1:T(8,128)(2,1)}, u32[]{:S(2)}) copy-start(bf16[4096,64]{0,1:T(8,128)(2,1)} %param.21) | copy-start | bytes 1572868
  51.6 228.5 %reduce-scatter.2.cloned.1.call-start = ((), (), s32[]{:S(2)}) async-start(), calls=%async_computation.3 | async-start | bytes 4718592 | tf_op jit(solution)/shard_map/reduce_scatter | solution.py:176
  51.6 4.3 %copy-start.2 = (bf16[512,4096]{1,0:T(8,128)(2,1)S(1)}, bf16[512,4096]{1,0:T(8,128)(2,1)}, u32[]{:S(2)}) copy-start(bf16[512,4096]{1,0:T(8,128)(2,1)} %all-gather.3.cloned.1.call-done) | copy-start | bytes 12582916
  52.1 8.5 %copy-start.10 = (bf16[4096,256]{1,0:T(8,128)(2,1)S(1)}, bf16[4096,256]{1,0:T(8,128)(2,1)}, u32[]{:S(2)}) copy-start(bf16[4096,256]{1,0:T(8,128)(2,1)} %param.20) | copy-start | bytes 6291460
  57.4 4.6 %copy-start.11 = (bf16[4096,256]{1,0:T(8,128)(2,1)S(1)}, bf16[4096,256]{1,0:T(8,128)(2,1)}, u32[]{:S(2)}) copy-start(bf16[4096,256]{1,0:T(8,128)(2,1)} %param.17) | copy-start | bytes 6291460
  57.4 6.6 %collective-permute-start = (bf16[128,128]{0,1:T(8,128)(2,1)S(1)}, bf16[128,128]{0,1:T(8,128)(2,1)S(1)}, u32[]{:S(2)}, u32[]{:S(2)}) collective-permute-start(bf16[128,128]{0,1:T(8,128)(2,1)S(1)} %pad_maximum_fusion.1), channel_id=1, source_target_pairs={{0,8},{8,16},{16,24},{24,32},{32,40},{40,48},{48,56},{56,64},{64,7... | collective-permute-start | bytes 98312 | tf_op jit(solution)/shard_map/ppermute | solution.py:21
  64.0 1.1 copy-start.8
  139.6 31.4 %copy-start.6 = (f32[2]{0:T(128)S(1)}, f32[2]{0:T(128)}, u32[]{:S(2)}) copy-start(f32[2]{0:T(128)} %param.23) | copy-start | bytes 28
  139.6 31.7 %copy-start.7 = (f32[128]{0:T(128)S(1)}, f32[128]{0:T(128)}, u32[]{:S(2)}) copy-start(f32[128]{0:T(128)} %param.24) | copy-start | bytes 1540
  171.4 1.6 copy-start.3
Sparse Core Ops, SparseCore 0:
  9.0 35.6 all-gather.2
  51.7 75.5 all-gather.4
  176.4 103.6 reduce-scatter.1
where the time goes:
time: 290 us; the launch traced here: 287 us
  waiting for transfers between devices  201 us (69%)
  matrix products  28.8 us (10%)
  local copies, waits for them, and re-layouts  23 us (8%)
  between operations  13.4 us (5%)
  loops' own time  11.3 us (4%)
  other arithmetic  5.89 us (2%)
  starting transfers between devices  3.32 us (1%)
    reduce_scatter x1, waiting for transfers between devices, shards(): lax.psum_scatter((jnp.einsum('hqe,hen->qn', a_heads, a_weight, preferred_...  104 us
    all_gather x1, waiting for transfers between devices, side_by_side(): whole = lax.all_gather(both, axis, axis=dim, tiled=True)  59 us
    all_gather x1, waiting for transfers between devices, shards(): projected = project(lax.all_gather(inputs, 'tp', axis=0, tiled=True))  37.4 us
    dot_general x6, matrix products, project(): jnp.dot(shard_piece, matrix, preferred_element_type=jnp.float32)  14.1 us
    another operation x1, loops' own time, advance(): return lax.fori_loop(0, row_count // span_rows, one_span, states)  11.2 us
    while x1, local copies, waits for them, and re-layouts, advance(): return lax.fori_loop(0, row_count // span_rows, one_span, states)  6.32 us
    split x1, local copies, waits for them, and re-layouts, side_by_side(): jnp.split(whole, [sum(widths[:k]) for k in range(1, len(widths))], axis=a...  5.86 us
  transfers between devices with their start and end apart: 4, of which 3 were waited for; matrix products, arithmetic and copies ran while one was open for 5% of the time, Pallas kernels for 0%

commit v1 on v0

v1 whole, which is shorter than its diff:
```python
import functools

import jax
import jax.numpy as jnp
from jax import lax
from jax.experimental import pallas as pl
from jax.experimental.pallas import tpu as pltpu
from jax.sharding import PartitionSpec as P

HEAD_DIM = 64
VALUE_DIM = 128
WINDOW = 128

norm_eps = 0.0001
head_scale = 0.8
mask_fill = -1e30

MESH = pl.DeviceIdType.MESH
NT = (((1,), (1,)), ((), ()))
LOG2E = 1.4426950408889634
VMEM = pltpu.VMEM
F32 = jnp.float32
BF16 = jnp.bfloat16


def remote(src, dst, send_sem, recv_sem, row, col):
    return pltpu.make_async_remote_copy(
        src_ref=src,
        dst_ref=dst,
        send_sem=send_sem,
        recv_sem=recv_sem,
        device_id=(row, col),
        device_id_type=MESH,
    )


def soft_chunk(items, score, lookup, mx, ls, acc):
    def weights(i, pieces):
        before = mx[i]
        top = before
        for piece in pieces:
            top = jnp.maximum(top, jnp.max(piece, axis=0, keepdims=True))
        shrink = jnp.exp2(before - top)
        mx[i] = top
        return shrink, [jnp.exp2(piece - top).astype(BF16) for piece in pieces]

    def collect(i, shrink, pieces):
        got = jnp.dot(lookup, jnp.concatenate(pieces, axis=0), preferred_element_type=F32)
        acc[i] = acc[i] * shrink + got[:VALUE_DIM]
        ls[i] = ls[i] * shrink + got[VALUE_DIM : VALUE_DIM + 1]

    now = score(items[0])
    held = None
    for at, i in enumerate(items):
        later = score(items[at + 1]) if at + 1 < len(items) else None
        current = weights(i, now)
        if held is not None:
            collect(items[at - 1], *held)
        held, now = current, later
    collect(items[-1], *held)


def attention_kernel(
    q_in, kv_in, bq_in, bkv_in, lam_in, gain_in, sink_in,
    a_out, b_out,
    kv, q_raw, q_mul, near, lam, acc, mx, ls, stage, back,
    a2a_s, a2a_r, zs, zr, rs, rr, ds, dr, q_s, q_r, small_s, small_r, ret_s, ret_r,
):
    s, t = lax.axis_index("sp"), lax.axis_index("tp")
    z, y = s // 4, s % 4
    x, c = t // 2, t % 2
    other = 2 * x + 1 - c
    up, down = (z + 1) % 4, (z + 3) % 4
    far = (z + 2) % 4
    mate = 3 - z
    side = z + 1 - 2 * (z % 2)
    quarter = 2 * c + z // 2
    order = (y, y + 1 - 2 * (y % 2), 3 - y, (y + 2) % 4)

    barrier = pltpu.get_barrier_semaphore()

    def greet(row, col):
        pl.semaphore_signal(barrier, inc=1, device_id=(row, col), device_id_type=MESH)

    for j in range(4):
        for core in range(2):
            if j == 0:
                @pl.when(core != c)
                def _(core=core):
                    greet(4 * z + y, 2 * x + core)
            else:
                greet(4 * z + (y + j) % 4, 2 * x + core)
            greet(4 * mate + (y + j) % 4, 2 * x + core)
    greet(4 * side + y, t)
    rim_up = (y == 3) & (z % 2 == 0)
    rim_down = (y == 0) & (z % 2 == 1)

    @pl.when(rim_up)
    def _():
        greet(s + 1, t)

    @pl.when(rim_down)
    def _():
        greet(s - 1, t)

    pl.semaphore_wait(barrier, 16 + jnp.where(rim_up | rim_down, 1, 0))

    def kv_send(head, part):
        return remote(
            kv_in.at[head, part], kv.at[part, z, y], a2a_s.at[head, part], a2a_r.at[y],
            4 * z + 2 * c + head, 2 * x + part,
        )

    def kv_local(head, part):
        return (2 * c + head == y) & (part == c)

    def q_send(head, k, core):
        goal = z if k == 0 else mate
        return remote(
            q_in.at[head, pl.ds(128 * (2 * core + goal // 2), 128)], q_raw.at[z // 2, y],
            q_s.at[head, k, core], q_r.at[z // 2, y],
            4 * goal + 2 * c + head, 2 * x + core,
        )

    def q_local(head, k, core):
        return (2 * c + head == y) & (core == c) & (k == 0)

    for head in range(2):
        for part in range(2):
            @pl.when(~kv_local(head, part))
            def _(head=head, part=part):
                kv_send(head, part).start()

    lam_send = remote(lam_in, lam.at[c], small_s.at[0], small_r.at[0], s, other)
    lam_send.start()
    near_send = remote(
        bkv_in.at[pl.ds(384, 128)], near.at[pl.ds(0, 128)], small_s.at[1], small_r.at[1],
        jnp.minimum(s + 1, 15), t,
    )

    @pl.when(s < 15)
    def _():
        near_send.start()

    for head in range(2):
        for k in range(2):
            for core in range(2):
                @pl.when(~q_local(head, k, core))
                def _(head=head, k=k, core=core):
                    q_send(head, k, core).start()

    for head in range(2):
        @pl.when(2 * c + head == y)
        def _(head=head):
            kv[c, z, y] = kv_in[head, c]
            q_raw[z // 2, y] = q_in[head, pl.ds(128 * quarter, 128)]

    lam[c] = lam_in[...]

    def half(which):
        return pl.ds(256 * which, 256)

    def z_send(row, which, upward):
        return remote(
            kv.at[c, z, row, half(which)], kv.at[c, z, row, half(which)],
            zs.at[row, which, 0 if upward else 1], zr.at[row, which, 0 if upward else 1],
            4 * (up if upward else down) + y, t,
        )

    def z_wait(row, which, upward):
        level = down if upward else up
        return remote(
            kv.at[c, level, row, half(which)], kv.at[c, level, row, half(which)],
            zs.at[row, which, 0 if upward else 1], zr.at[row, which, 0 if upward else 1],
            4 * (up if upward else down) + y, t,
        )

    def relay_send(row, upward):
        level, which = (down, 0) if upward else (up, 1)
        return remote(
            kv.at[c, level, row, half(which)], kv.at[c, level, row, half(which)],
            rs.at[row, which], rr.at[row, which],
            4 * (up if upward else down) + y, t,
        )

    def relay_wait(row, which):
        return remote(
            kv.at[c, far, row, half(which)], kv.at[c, far, row, half(which)],
            rs.at[row, which], rr.at[row, which],
            4 * (up if which == 0 else down) + y, t,
        )

    def cross_send(level, row):
        return remote(
            kv.at[c, level, row], kv.at[c, level, row],
            ds.at[level, row], dr.at[level, row], s, other,
        )

    def cross_wait(level, row):
        return remote(
            kv.at[1 - c, level, row], kv.at[1 - c, level, row],
            ds.at[level, row], dr.at[level, row], s, other,
        )

    def a2a_wait(row):
        return remote(
            kv.at[c, z, row], kv.at[c, z, row], a2a_s.at[0, 0], a2a_r.at[row], s, other
        )

    def spread(row):
        z_send(row, 0, True).start()
        z_send(row, 1, False).start()
        z_send(row, 1, True).start()
        z_send(row, 0, False).start()
        cross_send(z, row).start()

    @pl.when(y // 2 != c)
    def _():
        a2a_wait(y).wait_recv()

    spread(order[0])
    acc[...] = jnp.zeros_like(acc)
    ls[...] = jnp.zeros_like(ls)
    mx[...] = jnp.full_like(mx, mask_fill)
    near[pl.ds(128, 512)] = bkv_in[...]

    @pl.when(s == 0)
    def _():
        near[pl.ds(0, 128)] = jnp.zeros((128, 128), BF16)

    a2a_wait(order[1]).wait_recv()
    spread(order[1])

    @pl.when(s > 0)
    def _():
        near_send.wait_recv()

    lane = lax.broadcasted_iota(jnp.int32, (1, 128), 1)

    def windowed(block, carry):
        start = pl.multiple_of(block * 128, 128)
        span = near[pl.ds(start, 256)]
        span32 = span.astype(F32)
        turned = jnp.concatenate([span32[:, HEAD_DIM:], span32[:, :HEAD_DIM]], axis=1)
        keys = jnp.where(lane < HEAD_DIM, span32, turned).astype(BF16)
        values = jnp.transpose(span32)[HEAD_DIM:].astype(BF16)
        parts = []
        sinks = []
        for j in range(4):
            own = bq_in[pl.ds(start, 128), 128 * (j // 2) : 128 * (j // 2 + 1)]
            mine = (lane >= HEAD_DIM) if j % 2 else (lane < HEAD_DIM)
            parts.append(jnp.where(mine, own.astype(F32), 0.0).astype(BF16))
            sinks.append(jnp.full((1, 128), sink_in[j] * LOG2E, F32))
        queries = jnp.concatenate(parts, axis=0)
        sink = jnp.concatenate(sinks, axis=1)
        scores = lax.dot_general(keys, queries, NT, preferred_element_type=F32)
        scores = scores * (LOG2E * HEAD_DIM ** (-0.5))
        key_at = lax.broadcasted_iota(jnp.int32, (256, 512), 0)
        query_at = lax.broadcasted_iota(jnp.int32, (256, 512), 1) % 128
        first = jnp.where((s == 0) & (block == 0), 128, 0)
        allowed = (key_at > query_at) & (key_at <= query_at + WINDOW) & (key_at >= first)
        scores = jnp.where(allowed, scores, mask_fill)
        top = jnp.maximum(jnp.max(scores, axis=0, keepdims=True), sink)
        weights = jnp.exp2(scores - top)
        total = jnp.sum(weights, axis=0, keepdims=True) + jnp.exp2(sink - top)
        found = jnp.dot(values, weights.astype(BF16), preferred_element_type=F32) / total
        tall = jnp.concatenate([found[:, 128 * j : 128 * (j + 1)] for j in range(4)], axis=0)
        b_out[pl.ds(start, 128)] = jnp.transpose(tall).astype(BF16)
        return carry

    lax.fori_loop(0, 4, windowed, 0)

    a2a_wait(order[2]).wait_recv()
    spread(order[2])
    a2a_wait(order[3]).wait_recv()
    spread(order[3])

    for pair in range(2):
        for row in range(4):
            @pl.when(~((pair == z // 2) & (row == y) & (y // 2 == c)))
            def _(pair=pair, row=row):
                remote(
                    q_raw.at[pair, row], q_raw.at[pair, row], q_s.at[0, 0, 0],
                    q_r.at[pair, row], s, other,
                ).wait_recv()

    for pair in range(2):
        for row in range(4):
            wide = q_raw[pair, row].astype(F32) * (LOG2E * HEAD_DIM ** (-0.5))
            high = wide.astype(BF16).astype(F32)
            low = wide - high
            for m in range(2):
                mine = (lane >= HEAD_DIM) if m else (lane < HEAD_DIM)
                i = pair * 4 + (row // 2) * 2 + m
                rows = slice(128 * (row % 2), 128 * (row % 2) + 128)
                q_mul[i, rows, 0:128] = jnp.where(mine, high, 0.0).astype(BF16)
                q_mul[i, rows, 128:256] = jnp.where(mine, low, 0.0).astype(BF16)

    def relay(row):
        z_wait(row, 0, True).wait_recv()
        relay_send(row, True).start()
        z_wait(row, 1, False).wait_recv()
        relay_send(row, False).start()
        z_wait(row, 1, True).wait_recv()
        cross_send(down, row).start()
        z_wait(row, 0, False).wait_recv()
        cross_send(up, row).start()

    def relay_far(row):
        relay_wait(row, 0).wait_recv()
        relay_wait(row, 1).wait_recv()
        cross_send(far, row).start()

    def load_pair(level, pair):
        keys = kv[0, level, pl.ds(2 * pair, 2)].reshape(1024, 128)
        held = kv[1, level, pl.ds(2 * pair, 2)].reshape(1024, 128)
        lookup = jnp.concatenate([held[128 * k : 128 * (k + 1)] for k in range(8)], axis=1)
        lookup = jnp.concatenate([lookup, jnp.ones((16, 1024), BF16)], axis=0)
        return jnp.concatenate([keys, keys], axis=1), lookup

    apart = lax.broadcasted_iota(jnp.int32, (256, 256), 0)
    column = lax.broadcasted_iota(jnp.int32, (256, 256), 1)
    apart = apart - (column % 128) - 512 * (column // 128)

    def attend(level, pair, sel):
        mark = jnp.where(sel == 0, jnp.minimum(z, mate), jnp.maximum(z, mate))

        @pl.when(level < mark)
        def _():
            keys, lookup = load_pair(level, pair)

            def score(i):
                return [
                    lax.dot_general(
                        keys[256 * k : 256 * (k + 1)], q_mul[i], NT, preferred_element_type=F32
                    )
                    for k in range(4)
                ]

            soft_chunk([sel * 4 + k for k in range(4)], score, lookup, mx, ls, acc)

        @pl.when(level == mark)
        def _():
            def group(g, carry):
                keys, lookup = load_pair(level, pair)
                base = 1024 * g + 128 * quarter - 1024 * pair

                def score(i):
                    return [
                        jnp.where(
                            apart <= base - 256 * k,
                            lax.dot_general(
                                keys[256 * k : 256 * (k + 1)], q_mul[i], NT,
                                preferred_element_type=F32,
                            ),
                            mask_fill,
                        )
                        for k in range(4)
                    ]

                first = sel * 4 + g * 2
                soft_chunk([first, first + 1], score, lookup, mx, ls, acc)
                return carry

            lax.fori_loop(pair, 2, group, 0)

    def step(it, carry):
        @pl.when((it >= 1) & (it <= 4))
        def _():
            j = it - 1
            row = jnp.where(
                j == 0, order[0], jnp.where(j == 1, order[1], jnp.where(j == 2, order[2], order[3]))
            )
            relay(row)

        @pl.when(it == 5)
        def _():
            relay_far(order[0])
            relay_far(order[1])

        @pl.when(it == 6)
        def _():
            relay_far(order[2])

        @pl.when(it == 7)
        def _():
            relay_far(order[3])

        below = (it == 2) | (it == 4)
        above = (it == 3) | (it == 5)
        level = jnp.where(it < 2, z, jnp.where(below, down, jnp.where(above, up, far)))
        near_pair = (it == 0) | (it == 2) | (it == 3) | (it == 6)
        pair = jnp.where(near_pair, y // 2, 1 - y // 2)
        cross_wait(level, 2 * pair).wait_recv()
        cross_wait(level, 2 * pair + 1).wait_recv()

        def one(sel, inner):
            attend(level, pair, sel)
            return inner

        lax.fori_loop(0, 2, one, 0)
        return carry

    lax.fori_loop(0, 8, step, 0)

    lam_send.wait_recv()
    mixing = lam[y // 2, y % 2, 0:1, :]
    gain = gain_in[...] * head_scale

    def ret_send(pair, row):
        goal = jnp.minimum(z, mate) if pair == 0 else jnp.maximum(z, mate)
        return remote(
            stage.at[pair, row], back.at[y % 2, pl.ds(128 * quarter, 128)],
            ret_s.at[pair, row], ret_r.at[y % 2, quarter],
            4 * goal + row, 2 * x + y // 2,
        )

    def ret_local(pair, row):
        return (pair == z // 2) & (row == y) & (y // 2 == c)

    for pair in range(2):
        for g in range(2):
            i = pair * 4 + g * 2
            first = acc[i] / ls[i]
            second = acc[i + 1] / ls[i + 1]
            gap = first - mixing * second
            square = jnp.mean(gap * gap, axis=0, keepdims=True)
            done = gap * lax.rsqrt(square + norm_eps) * gain
            rows = jnp.transpose(done).astype(BF16)
            for k in range(2):
                row = 2 * g + k
                stage[pair, row] = rows[128 * k : 128 * (k + 1)]

                @pl.when(~ret_local(pair, row))
                def _(pair=pair, row=row):
                    ret_send(pair, row).start()

                @pl.when(ret_local(pair, row))
                def _(pair=pair, row=row):
                    back[y % 2, pl.ds(128 * quarter, 128)] = stage[pair, row]

    for head in range(2):
        for part in range(2):
            @pl.when(~kv_local(head, part))
            def _(head=head, part=part):
                kv_send(head, part).wait_send()
        for k in range(2):
            for core in range(2):
                @pl.when(~q_local(head, k, core))
                def _(head=head, k=k, core=core):
                    q_send(head, k, core).wait_send()
    lam_send.wait_send()

    @pl.when(s < 15)
    def _():
        near_send.wait_send()

    def drain(row, carry):
        for which in range(2):
            for upward in (True, False):
                z_send(row, which, upward).wait_send()
        relay_send(row, True).wait_send()
        relay_send(row, False).wait_send()
        for level in range(4):
            cross_send(level, row).wait_send()
        return carry

    lax.fori_loop(0, 4, drain, 0)
    for head in range(2):
        for part in range(4):
            mine = (2 * c + head == y) & (part == quarter)

            @pl.when(~mine)
            def _(head=head, part=part):
                spot = back.at[head, pl.ds(128 * part, 128)]
                remote(spot, spot, ret_s.at[0, 0], ret_r.at[head, part], s, other).wait_recv()

    a_out[...] = back[...]
    for pair in range(2):
        for row in range(4):
            @pl.when(~ret_local(pair, row))
            def _(pair=pair, row=row):
                ret_send(pair, row).wait_send()


def attention(q_in, kv_in, bq_in, bkv_in, lam_in, gain_in, sink_in):
    vmem = pl.BlockSpec(memory_space=VMEM)
    dma = pltpu.SemaphoreType.DMA
    return pl.pallas_call(
        attention_kernel,
        out_shape=(
            jax.ShapeDtypeStruct((2, 512, 128), BF16),
            jax.ShapeDtypeStruct((512, 256), BF16),
        ),
        in_specs=[vmem] * 6 + [pl.BlockSpec(memory_space=pltpu.SMEM)],
        out_specs=(vmem, vmem),
        scratch_shapes=[
            VMEM((2, 4, 4, 512, 128), BF16),
            VMEM((2, 4, 128, 128), BF16),
            VMEM((8, 256, 256), BF16),
            VMEM((640, 128), BF16),
            VMEM((2, 2, 8, 256), F32),
            VMEM((8, 128, 256), F32),
            VMEM((8, 1, 256), F32),
            VMEM((8, 1, 256), F32),
            VMEM((2, 4, 128, 128), BF16),
            VMEM((2, 512, 128), BF16),
            dma((2, 2)), dma((4,)),
            dma((4, 2, 2)), dma((4, 2, 2)),
            dma((4, 2)), dma((4, 2)),
            dma((4, 4)), dma((4, 4)),
            dma((2, 2, 2)), dma((2, 4)),
            dma((2,)), dma((2,)),
            dma((2, 4)), dma((2, 4)),
        ],
        compiler_params=pltpu.CompilerParams(
            collective_id=1, has_side_effects=True, vmem_limit_bytes=50 * 2**20
        ),
        name="attention",
    )(q_in, kv_in, bq_in, bkv_in, lam_in, gain_in, sink_in)


def shards(
    inputs,
    a_query_w,
    a_key_w,
    a_value_w,
    b_query_w,
    b_key_w,
    b_value_w,
    head_lambda,
    head_gain,
    sink_logit,
    a_out_w,
    b_out_w,
):
    rows = lax.all_gather(inputs, "tp", axis=0, tiled=True)

    def project(matrix):
        return jnp.dot(rows, matrix, preferred_element_type=F32).astype(BF16)

    q = project(a_query_w).reshape(512, 2, 128).transpose(1, 0, 2)
    k = project(a_key_w).reshape(512, 2, 128).transpose(1, 0, 2)
    v = project(a_value_w).reshape(4, 128, 2, 128).transpose(2, 0, 3, 1).reshape(2, 512, 128)
    kv = jnp.stack([k, v], axis=1)
    bq = project(b_query_w)
    bkv = jnp.concatenate([project(b_key_w), project(b_value_w)], axis=1)
    lam = jnp.broadcast_to(head_lambda[:, None, None], (2, 8, 256))
    a_heads, b_heads = attention(q, kv, bq, bkv, lam, head_gain[:, None], sink_logit)
    a_weight = a_out_w.reshape(2, VALUE_DIM, 4096)
    return lax.psum_scatter(
        (
            jnp.einsum("hqe,hen->qn", a_heads, a_weight, preferred_element_type=F32)
            + jnp.dot(b_heads, b_out_w, preferred_element_type=F32)
        ).astype(BF16),
        "tp",
        scatter_dimension=0,
        tiled=True,
    )


def solution(mesh):
    return jax.shard_map(
        shards,
        mesh=mesh,
        in_specs=(
            P(("sp", "tp"), None),
            P(None, "tp"),
            P(None, "tp"),
            P(None, "tp"),
            P(None, "tp"),
            P(None, "tp"),
            P(None, "tp"),
            P("tp"),
            P(),
            P("tp"),
            P("tp", None),
            P("tp", None),
        ),
        out_specs=P(("sp", "tp"), None),
        check_vma=False,
    )
```

time: 290 us -> 163 us (0.56)
  waiting for transfers between devices: 201 us -> 71.6 us
  Pallas kernels: 0 us -> 44.7 us
  local copies, waits for them, and re-layouts: 23 us -> 2.04 us
  loops' own time: 11.3 us -> 0 us
  other arithmetic: 5.89 us -> 0.16 us
  starting transfers between devices: 3.32 us -> 0.04 us
    reduce_scatter x1, waiting for transfers between devices: 104 us -> 34.3 us  [shards(): lax.psum_scatter((jnp.einsum('hqe,hen->qn', a_heads, a_weight, preferred_...]
    all_gather x2 -> x1, waiting for transfers between devices: 96.3 us -> 36.6 us  [shards(): rows = lax.all_gather(inputs, 'tp', axis=0, tiled=True)]
    pallas_call x0 -> x1, Pallas kernels: none -> 44.7 us  [attention(): pl.pallas_call(attention_kernel, out_shape=(jax.ShapeDtypeStruct((2, 512,...]
    another operation x9 -> x0, loops' own time: 11.3 us -> none  [the longest x1 11.2 us: advance(): return lax.fori_loop(0, row_count // span_rows, one_span, states)]
    slice x16 -> x0, local copies, waits for them, and re-layouts: 9.95 us -> none  [the longest x8 5.18 us: one_span(): query_pos[-1]]
    while x1 -> x0, local copies, waits for them, and re-layouts: 6.32 us -> none  [advance(): return lax.fori_loop(0, row_count // span_rows, one_span, states)]
    split x1 -> x0, local copies, waits for them, and re-layouts: 5.86 us -> none  [side_by_side(): jnp.split(whole, [sum(widths[:k]) for k in range(1, len(widths))], axis=a...]
    reduce_sum x3 -> x0, other arithmetic: 3.69 us -> none  [the longest x1 2.1 us: attend_block(): totals = totals * shrink + jnp.sum(weights, axis=-1)]
  transfers between devices with their start and end apart: 4 -> 2, of which waited for: 3 -> 2; matrix products, arithmetic and copies ran while one was open for 5% -> 0% of each run, Pallas kernels for 0% -> 0%
where the time goes in v1:
time: 163 us; the launch traced here: 161 us
  waiting for transfers between devices  71.6 us (44%)
  Pallas kernels  44.7 us (27%)
  matrix products  28.4 us (17%)
  between operations  13.5 us (8%)
  local copies, waits for them, and re-layouts  2.04 us (1%)
    pallas_call x1, Pallas kernels, attention(): pl.pallas_call(attention_kernel, out_shape=(jax.ShapeDtypeStruct((2, 512,...  44.7 us
    all_gather x1, waiting for transfers between devices, shards(): rows = lax.all_gather(inputs, 'tp', axis=0, tiled=True)  36.6 us
    reduce_scatter x1, waiting for transfers between devices, shards(): lax.psum_scatter((jnp.einsum('hqe,hen->qn', a_heads, a_weight, preferred_...  34.3 us
    dot_general x6, matrix products, project(): return jnp.dot(rows, matrix, preferred_element_type=F32).astype(BF16)  23.8 us
    dot_general x1, matrix products, shards(): jnp.dot(b_heads, b_out_w, preferred_element_type=F32)  3.29 us
  transfers between devices with their start and end apart: 2, of which 2 were waited for; matrix products, arithmetic and copies ran while one was open for 0% of the time, Pallas kernels for 0%

profile of v1, /device:TPU:1, one launch (start us, length us, event | category | flops | bytes accessed | tf_op | source)
XLA Modules:
  0.0 160.5 jit_solution(4576896294899005430)
XLA Ops:
  6.5 0.0 copy-start
  6.5 0.0 all-gather.2.cloned.1.call-start
  6.5 0.7 all-gather.2.cloned.1.call-update
  7.3 0.0 reduce-scatter.2.cloned.1.call-start
  7.3 0.8 copy.28.gain_in
  8.1 36.6 %all-gather.2.cloned.1.call-done = bf16[512,4096]{1,0:T(8,128)(2,1)} async-done(((bf16[64,4096]{1,0:T(8,128)(2,1)}), bf16[512,4096]{1,0:T(8,128)(2,1)}) %all-gather.2.cloned.1.call-update) | async-done | bytes 4194320 | tf_op jit(solution)/shard_map/all_gather | solution.py:537
  44.7 3.7 %convolution_convert_fusion.4 = bf16[512,64]{0,1:T(8,128)(2,1)S(1)} fusion(bf16[512,4096]{1,0:T(8,128)(2,1)} %all-gather.2.cloned.1.call-done, bf16[4096,64]{0,1:T(8,128)(2,1)} %param.18), kind=kOutput, calls=%fused_computation.6 | convolution fusion | flops 268468224 | bytes 4784128 | tf_op jit(solution)/shard_map/dot_general | solution.py:540
  48.4 0.1 copy.27
  48.5 0.0 copy-done.3
  48.5 3.6 %convolution_convert_fusion.5 = bf16[512,64]{0,1:T(8,128)(2,1)S(1)} fusion(bf16[512,4096]{1,0:T(8,128)(2,1)} %all-gather.2.cloned.1.call-done, bf16[4096,64]{0,1:T(8,128)(2,1)S(1)} %copy-done.3), kind=kOutput, calls=%fused_computation.7 | convolution fusion | flops 268468224 | bytes 4784128 | tf_op jit(solution)/shard_map/dot_general | solution.py:540
  52.1 0.1 copy.26
  52.2 4.1 %convolution_convert_fusion.1 = bf16[512,256]{1,0:T(8,128)(2,1)S(1)} fusion(bf16[512,4096]{1,0:T(8,128)(2,1)} %all-gather.2.cloned.1.call-done, bf16[4096,256]{1,0:T(8,128)(2,1)} %param.15), kind=kOutput, calls=%fused_computation.3 | convolution fusion | flops 1073872896 | bytes 6553600 | tf_op jit(solution)/shard_map/dot_general | solution.py:540
  56.4 0.1 reshape.15
  56.4 0.2 copy.25
  56.6 4.2 %convolution_convert_fusion.3 = bf16[512,256]{0,1:T(8,128)(2,1)S(1)} fusion(bf16[512,4096]{1,0:T(8,128)(2,1)} %all-gather.2.cloned.1.call-done, bf16[4096,256]{1,0:T(8,128)(2,1)} %param.13), kind=kOutput, calls=%fused_computation.5 | convolution fusion | flops 1073872896 | bytes 6553600 | tf_op jit(solution)/shard_map/dot_general | solution.py:540
  60.8 0.2 copy.23
  61.0 4.2 %convolution_convert_fusion.2 = bf16[512,256]{0,1:T(8,128)(2,1)S(1)} fusion(bf16[512,4096]{1,0:T(8,128)(2,1)} %all-gather.2.cloned.1.call-done, bf16[4096,256]{1,0:T(8,128)(2,1)} %param.14), kind=kOutput, calls=%fused_computation.4 | convolution fusion | flops 1073872896 | bytes 6553600 | tf_op jit(solution)/shard_map/dot_general | solution.py:540
  65.2 0.2 copy.24
  65.3 0.1 pad_maximum_fusion.1.bkv_in
  65.5 0.1 pad_maximum_fusion.kv_in
  65.5 0.0 copy-start.4
  65.5 0.0 copy-start.1
  65.5 4.1 %convolution_convert_fusion.bq_in = bf16[512,256]{1,0:T(8,128)(2,1)S(1)} fusion(bf16[512,4096]{1,0:T(8,128)(2,1)} %all-gather.2.cloned.1.call-done, bf16[4096,256]{1,0:T(8,128)(2,1)} %param.16), kind=kOutput, calls=%fused_computation.2 | convolution fusion | flops 1073872896 | bytes 6553600 | tf_op jit(solution)/shard_map/dot_general | solution.py:540
  69.7 0.1 broadcast_in_dim.4.lam_in
  69.7 44.7 %attention.1 = (bf16[2,512,128]{2,1,0:T(8,128)(2,1)S(1)}, bf16[512,256]{1,0:T(8,128)(2,1)S(1)}) custom-call(bf16[2,512,128]{2,1,0:T(8,128)(2,1)S(1)} %bitcast.32, bf16[2,2,512,128]{3,2,1,0:T(8,128)(2,1)S(1)} %pad_maximum_fusion.kv_in, bf16[512,256]{1,0:T(8,128)(2,1)S(1)} %convolution_convert_fusion.bq_in, bf16[512,128]{1,0:T(8,128)(2,1)S(1)} %pad_maximum_fusion.1.bkv_in, ...), custom_call_target="tpu_custom_call" | custom-call | tf_op jit(solution)/shard_map/attention/pallas_call | solution.py:489
  114.4 0.0 copy-done
  114.5 0.0 copy-start.2
  114.5 1.3 fusion.1
  115.7 0.3 copy-done.2
  116.1 3.3 %fusion = bf16[512,4096]{1,0:T(8,128)(2,1)} fusion(f32[512,4096,1]{1,0,2:T(8,128)S(1)} %fusion.1, bf16[512,256]{1,0:T(8,128)(2,1)S(1)} %get-tuple-element.8, bf16[256,4096]{1,0:T(8,128)(2,1)S(1)} %copy-done.2), kind=kOutput, calls=%fused_computation.1 | convolution fusion | flops 1077936128 | bytes 14942208 | tf_op jit(solution)/shard_map/dot_general | solution.py:554
  119.3 0.0 reduce-scatter.2.cloned.1.call-update
  119.4 34.3 %reduce-scatter.2.cloned.1.call-done = bf16[64,4096]{1,0:T(8,128)(2,1)} async-done(((bf16[512,4096]{1,0:T(8,128)(2,1)}), bf16[64,4096]{1,0:T(8,128)(2,1)}) %reduce-scatter.2.cloned.1.call-update) | async-done | bytes 524304 | tf_op jit(solution)/shard_map/reduce_scatter | solution.py:551
  (3 shorter events, 0.0 us)
Async XLA Ops:
  6.5 107.9 %copy-start = (bf16[256,4096]{1,0:T(8,128)(2,1)S(1)}, bf16[256,4096]{1,0:T(8,128)(2,1)}, u32[]{:S(2)}) copy-start(bf16[256,4096]{1,0:T(8,128)(2,1)} %param.22) | copy-start | bytes 6291460
  6.5 42.0 %copy-start.3 = (bf16[4096,64]{0,1:T(8,128)(2,1)S(1)}, bf16[4096,64]{0,1:T(8,128)(2,1)}, u32[]{:S(2)}) copy-start(bf16[4096,64]{0,1:T(8,128)(2,1)} %param.17) | copy-start | bytes 1572868
  6.5 38.2 %all-gather.2.cloned.1.call-start = ((), (), s32[]{:S(2)}) async-start(), calls=%async_computation.1 | async-start | bytes 4718592 | tf_op jit(solution)/shard_map/all_gather | solution.py:537
  7.3 146.4 %reduce-scatter.2.cloned.1.call-start = ((), (), s32[]{:S(2)}) async-start(), calls=%async_computation.2 | async-start | bytes 4718592 | tf_op jit(solution)/shard_map/reduce_scatter | solution.py:551
  65.5 4.2 %copy-start.4 = (f32[2]{0:T(128)S(1)}, f32[2]{0:T(128)}, u32[]{:S(2)}) copy-start(f32[2]{0:T(128)} %param.19) | copy-start | bytes 28
  65.5 4.2 %copy-start.1 = (f32[4]{0:T(128)S(1)}, f32[4]{0:T(128)}, u32[]{:S(2)}) copy-start(f32[4]{0:T(128)} %sink_in.1) | copy-start | bytes 52
  114.5 1.6 copy-start.2
Sparse Core Ops, SparseCore 0:
  9.0 35.6 all-gather.1
  119.5 34.1 reduce-scatter.1

commit v2 on v1

--- a/solution.py
+++ b/solution.py
@@ -520,6 +520,311 @@
     )(q_in, kv_in, bq_in, bkv_in, lam_in, gain_in, sink_in)
 
 
+NC = 8
+CW = 512
+
+
+def output_kernel(
+    a_in, b_in, aw_in, bw_in, out,
+    weights, part, crossed, chip, far_l, far_r, got_l, got_r, relayed,
+    w_s, cr_s, cr_r, fs, fr, gs, gr,
+):
+    s, t = lax.axis_index("sp"), lax.axis_index("tp")
+    x, c = t // 2, t % 2
+    xr, xl, xf = (x + 1) % 4, (x + 3) % 4, (x + 2) % 4
+    other, right, left = 2 * x + 1 - c, 2 * xr + c, 2 * xl + c
+
+    def fetch(n, which):
+        columns = pl.ds(pl.multiple_of(n * CW, CW), CW)
+        source = aw_in if which == 0 else bw_in
+        return pltpu.make_async_copy(
+            source.at[:, columns], weights.at[n, pl.ds(256 * which, 256)], w_s.at[n, which]
+        )
+
+    for n in range(NC):
+        fetch(n, 0).start()
+        fetch(n, 1).start()
+    barrier = pltpu.get_barrier_semaphore()
+    for col in (other, right, left):
+        pl.semaphore_signal(barrier, inc=1, device_id=(s, col), device_id_type=MESH)
+    pl.semaphore_wait(barrier, 3)
+
+    heads = jnp.concatenate([a_in[0], a_in[1], b_in[...]], axis=1)
+    first, second = pl.ds(0, 32), pl.ds(32, 32)
+
+    def cross(n):
+        return remote(part.at[n, 1 - c], crossed.at[n], cr_s.at[n], cr_r.at[n], s, other)
+
+    def far_send(n, way):
+        rows = first if way == 0 else second
+        return remote(
+            chip.at[n, xf, rows], (far_l if way == 0 else far_r).at[n],
+            fs.at[n, way], fr.at[n, way], s, right if way == 0 else left,
+        )
+
+    def near_send(n, way):
+        rows = second if way == 0 else first
+        return remote(
+            chip.at[n, xr if way == 0 else xl, rows], (got_l if way == 0 else got_r).at[n, rows],
+            gs.at[n, way, 0], gr.at[n, way, 0], s, right if way == 0 else left,
+        )
+
+    def sum_send(n, way):
+        rows = first if way == 0 else second
+        return remote(
+            relayed.at[n, way], (got_l if way == 0 else got_r).at[n, rows],
+            gs.at[n, way, 1], gr.at[n, way, 1], s, right if way == 0 else left,
+        )
+
+    def multiply(n):
+        fetch(n, 0).wait()
+        fetch(n, 1).wait()
+        partial = jnp.dot(heads, weights[n], preferred_element_type=F32).astype(BF16)
+        for col in range(8):
+            part[n, col % 2, col // 2] = partial[64 * col : 64 * (col + 1)]
+        cross(n).start()
+
+    def join(n):
+        cross(n).wait_recv()
+        chip[n] = (part[n, c].astype(F32) + crossed[n].astype(F32)).astype(BF16)
+        far_send(n, 0).start()
+        far_send(n, 1).start()
+        near_send(n, 0).start()
+        near_send(n, 1).start()
+
+    def pass_on(n, carry):
+        far_send(n, 0).wait_recv()
+        relayed[n, 0] = (chip[n, xr, first].astype(F32) + far_l[n].astype(F32)).astype(BF16)
+        sum_send(n, 0).start()
+        far_send(n, 1).wait_recv()
+        relayed[n, 1] = (chip[n, xl, second].astype(F32) + far_r[n].astype(F32)).astype(BF16)
+        sum_send(n, 1).start()
+        return carry
+
+    multiply(0)
+
+    def run(n, carry):
+        multiply(n)
+        join(n - 1)
+        return carry
+
+    lax.fori_loop(1, NC, run, 0)
+    join(NC - 1)
+    lax.fori_loop(0, NC, pass_on, 0)
+
+    for n in range(NC):
+        for way in range(2):
+            near_send(n, way).wait_recv()
+            sum_send(n, way).wait_recv()
+        total = chip[n, x].astype(F32) + got_l[n].astype(F32) + got_r[n].astype(F32)
+        out[:, n * CW : (n + 1) * CW] = total.astype(BF16)
+
+    def drain(n, carry):
+        cross(n).wait_send()
+        for way in range(2):
+            far_send(n, way).wait_send()
+            near_send(n, way).wait_send()
+            sum_send(n, way).wait_send()
+        return carry
+
+    lax.fori_loop(0, NC, drain, 0)
+
+
+def output(a_heads, b_heads, a_out_w, b_out_w):
+    vmem = pl.BlockSpec(memory_space=VMEM)
+    hbm = pl.BlockSpec(memory_space=pl.ANY)
+    dma = pltpu.SemaphoreType.DMA
+    return pl.pallas_call(
+        output_kernel,
+        out_shape=jax.ShapeDtypeStruct((64, 4096), BF16),
+        in_specs=[vmem, vmem, hbm, hbm],
+        out_specs=vmem,
+        scratch_shapes=[
+            VMEM((NC, 512, CW), BF16),
+            VMEM((NC, 2, 4, 64, CW), BF16),
+            VMEM((NC, 4, 64, CW), BF16),
+            VMEM((NC, 4, 64, CW), BF16),
+            VMEM((NC, 32, CW), BF16),
+            VMEM((NC, 32, CW), BF16),
+            VMEM((NC, 64, CW), BF16),
+            VMEM((NC, 64, CW), BF16),
+            VMEM((NC, 2, 32, CW), BF16),
+            dma((NC, 2)), dma((NC,)), dma((NC,)),
+            dma((NC, 2)), dma((NC, 2)), dma((NC, 2, 2)), dma((NC, 2, 2)),
+        ],
+        compiler_params=pltpu.CompilerParams(
+            collective_id=2, has_side_effects=True, vmem_limit_bytes=50 * 2**20
+        ),
+        name="output",
+    )(a_heads, b_heads, a_out_w, b_out_w)
+
+
+KC = 4
+KW = 1024
+WIDTHS = (256, 256, 256, 256, 64, 64)
+
+
+def project_kernel(
+    x_in, w0, w1, w2, w3, w4, w5, q_out, kv_out, bq_out, bkv_out,
+    rows, m0, m1, m2, m3, m4, m5, t0, t1, t2, t3, t4, t5,
+    w_s, os, orr, rs, rr, ds, dr,
+):
+    s, t = lax.axis_index("sp"), lax.axis_index("tp")
+    x, c = t // 2, t % 2
+    xr, xl, xf = (x + 1) % 4, (x + 3) % 4, (x + 2) % 4
+    other, right, left = 2 * x + 1 - c, 2 * xr + c, 2 * xl + c
+    beyond = 2 * xf + c
+    sources = (w0, w1, w2, w3, w4, w5)
+    mats = (m0, m1, m2, m3, m4, m5)
+    sums = (t0, t1, t2, t3, t4, t5)
+
+    def fetch(k, i):
+        return pltpu.make_async_copy(
+            sources[i].at[pl.ds(pl.multiple_of(k * KW, KW), KW)], mats[i].at[k], w_s.at[k, i]
+        )
+
+    for k in range(KC):
+        for i in range(6):
+            fetch(k, i).start()
+    barrier = pltpu.get_barrier_semaphore()
+    for col in (other, right, left):
+        pl.semaphore_signal(barrier, inc=1, device_id=(s, col), device_id_type=MESH)
+    pl.semaphore_wait(barrier, 3)
+
+    halves = (pl.ds(0, 32), pl.ds(32, 32))
+
+    def columns(k):
+        return pl.ds(pl.multiple_of(k * KW, KW), KW)
+
+    def own_send(k, way, which):
+        return remote(
+            x_in.at[halves[which], columns(k)], rows.at[k, t, halves[which]],
+            os.at[k, way, which], orr.at[k, way, which], s, right if way == 0 else left,
+        )
+
+    def own_wait(k, way, which):
+        spot = rows.at[k, left if way == 0 else right, halves[which]]
+        return remote(
+            spot, spot, os.at[k, way, which], orr.at[k, way, which],
+            s, right if way == 0 else left,
+        )
+
+    def relay_send(k, way):
+        spot = rows.at[k, left if way == 0 else right, halves[way]]
+        return remote(
+            spot, spot, rs.at[k, way], rr.at[k, way], s, right if way == 0 else left
+        )
+
+    def relay_wait(k, way):
+        spot = rows.at[k, beyond, halves[way]]
+        return remote(
+            spot, spot, rs.at[k, way], rr.at[k, way], s, right if way == 0 else left
+        )
+
+    def own_cross(k):
+        return remote(
+            x_in.at[:, columns(k)], rows.at[k, t], ds.at[k, x], dr.at[k, x], s, other
+        )
+
+    def cross(k, chip):
+        spot = rows.at[k, 2 * chip + c]
+        return remote(spot, spot, ds.at[k, chip], dr.at[k, chip], s, other)
+
+    def cross_wait(k, chip):
+        spot = rows.at[k, 2 * chip + 1 - c]
+        return remote(spot, spot, ds.at[k, chip], dr.at[k, chip], s, other)
+
+    for k in range(KC):
+        own_send(k, 0, 0).start()
+        own_send(k, 1, 1).start()
+        own_send(k, 0, 1).start()
+        own_send(k, 1, 0).start()
+        own_cross(k).start()
+    for k in range(KC):
+        rows[k, t] = x_in[:, k * KW : (k + 1) * KW]
+    for total in sums:
+        total[...] = jnp.zeros_like(total)
+
+    def pass_on(k, carry):
+        own_wait(k, 0, 0).wait_recv()
+        relay_send(k, 0).start()
+        own_wait(k, 1, 1).wait_recv()
+        relay_send(k, 1).start()
+        own_wait(k, 0, 1).wait_recv()
+        cross(k, xl).start()
+        own_wait(k, 1, 0).wait_recv()
+        cross(k, xr).start()
+        return carry
+
+    lax.fori_loop(0, KC, pass_on, 0)
+
+    def multiply(k, carry):
+        relay_wait(k, 0).wait_recv()
+        relay_wait(k, 1).wait_recv()
+        cross(k, xf).start()
+        for i in range(6):
+            fetch(k, i).wait()
+        for chip in (x, xl, xr, xf):
+            cross_wait(k, chip).wait_recv()
+        block = rows[k].reshape(512, KW)
+        for i in range(6):
+            sums[i][...] += jnp.dot(block, mats[i][k], preferred_element_type=F32)
+        return carry
+
+    lax.fori_loop(0, KC, multiply, 0)
+
+    for head in range(2):
+        lanes = slice(128 * head, 128 * (head + 1))
+        q_out[head] = t0[:, lanes].astype(BF16)
+        kv_out[head, 0] = t1[:, lanes].astype(BF16)
+        for j in range(4):
+            turned = jnp.transpose(t2[128 * j : 128 * (j + 1), lanes])
+            kv_out[head, 1, 128 * j : 128 * (j + 1)] = turned.astype(BF16)
+    bq_out[...] = t3[...].astype(BF16)
+    bkv_out[...] = jnp.concatenate([t4[...], t5[...]], axis=1).astype(BF16)
+
+    def drain(k, carry):
+        for way in range(2):
+            own_send(k, way, 0).wait_send()
+            own_send(k, way, 1).wait_send()
+            relay_send(k, way).wait_send()
+        own_cross(k).wait_send()
+        for chip in (xl, xr, xf):
+            cross(k, chip).wait_send()
+        return carry
+
+    lax.fori_loop(0, KC, drain, 0)
+
+
+def project(inputs, *matrices):
+    vmem = pl.BlockSpec(memory_space=VMEM)
+    hbm = pl.BlockSpec(memory_space=pl.ANY)
+    dma = pltpu.SemaphoreType.DMA
+    return pl.pallas_call(
+        project_kernel,
+        out_shape=(
+            jax.ShapeDtypeStruct((2, 512, 128), BF16),
+            jax.ShapeDtypeStruct((2, 2, 512, 128), BF16),
+            jax.ShapeDtypeStruct((512, 256), BF16),
+            jax.ShapeDtypeStruct((512, 128), BF16),
+        ),
+        in_specs=[vmem] + [hbm] * 6,
+        out_specs=(vmem,) * 4,
+        scratch_shapes=[VMEM((KC, 8, 64, KW), BF16)]
+        + [VMEM((KC, KW, width), BF16) for width in WIDTHS]
+        + [VMEM((512, width), F32) for width in WIDTHS]
+        + [
+            dma((KC, 6)),
+            dma((KC, 2, 2)), dma((KC, 2, 2)), dma((KC, 2)), dma((KC, 2)),
+            dma((KC, 4)), dma((KC, 4)),
+        ],
+        compiler_params=pltpu.CompilerParams(
+            collective_id=0, has_side_effects=True, vmem_limit_bytes=50 * 2**20
+        ),
+        name="project",
+    )(inputs, *matrices)
+
+
 def shards(
     inputs,
     a_query_w,
@@ -534,29 +839,12 @@
     a_out_w,
     b_out_w,
 ):
-    rows = lax.all_gather(inputs, "tp", axis=0, tiled=True)
-
-    def project(matrix):
-        return jnp.dot(rows, matrix, preferred_element_type=F32).astype(BF16)
-
-    q = project(a_query_w).reshape(512, 2, 128).transpose(1, 0, 2)
-    k = project(a_key_w).reshape(512, 2, 128).transpose(1, 0, 2)
-    v = project(a_value_w).reshape(4, 128, 2, 128).transpose(2, 0, 3, 1).reshape(2, 512, 128)
-    kv = jnp.stack([k, v], axis=1)
-    bq = project(b_query_w)
-    bkv = jnp.concatenate([project(b_key_w), project(b_value_w)], axis=1)
+    q, kv, bq, bkv = project(
+        inputs, a_query_w, a_key_w, a_value_w, b_query_w, b_key_w, b_value_w
+    )
     lam = jnp.broadcast_to(head_lambda[:, None, None], (2, 8, 256))
     a_heads, b_heads = attention(q, kv, bq, bkv, lam, head_gain[:, None], sink_logit)
-    a_weight = a_out_w.reshape(2, VALUE_DIM, 4096)
-    return lax.psum_scatter(
-        (
-            jnp.einsum("hqe,hen->qn", a_heads, a_weight, preferred_element_type=F32)
-            + jnp.dot(b_heads, b_out_w, preferred_element_type=F32)
-        ).astype(BF16),
-        "tp",
-        scatter_dimension=0,
-        tiled=True,
-    )
+    return output(a_heads, b_heads, a_out_w, b_out_w)
 
 
 def solution(mesh):

time: 163 us -> 110 us (0.67); the launches traced: 161 us -> 110 us
  waiting for transfers between devices: 71.6 us -> 0 us
  Pallas kernels: 44.7 us -> 103 us
  matrix products: 28.4 us -> 0 us
  between operations: 13.5 us -> 0.09 us
  local copies, waits for them, and re-layouts: 2.04 us -> 7.33 us
    pallas_call x0 -> x2, Pallas kernels: none -> 55.6 us  [the longest x1 30.9 us: project(): pl.pallas_call(project_kernel, out_shape=(jax.ShapeDtypeStruct((2, 512, 1...]
    all_gather x1 -> x0, waiting for transfers between devices: 36.6 us -> none  [shards(): rows = lax.all_gather(inputs, 'tp', axis=0, tiled=True)]
    reduce_scatter x1 -> x0, waiting for transfers between devices: 34.3 us -> none  [shards(): lax.psum_scatter((jnp.einsum('hqe,hen->qn', a_heads, a_weight, preferred_...]
    dot_general x8 -> x0, matrix products: 28.4 us -> none  [the longest x6 23.8 us: project(): return jnp.dot(rows, matrix, preferred_element_type=F32).astype(BF16)]
    unnamed x10 -> x17, local copies, waits for them, and re-layouts: 0.34 us -> 7.15 us
    pallas_call x1, Pallas kernels: 44.7 us -> 47 us  [attention(): pl.pallas_call(attention_kernel, out_shape=(jax.ShapeDtypeStruct((2, 512,...]
  transfers between devices with their start and end apart: 2 -> 0, of which waited for: 2 -> 0; matrix products, arithmetic and copies ran while one was open for 0% -> 0% of each run, Pallas kernels for 0% -> 0%
where the time goes in v2:
time: 110 us
  Pallas kernels  103 us (94%)
  local copies, waits for them, and re-layouts  7.33 us (7%)
    pallas_call x1, Pallas kernels, attention(): pl.pallas_call(attention_kernel, out_shape=(jax.ShapeDtypeStruct((2, 512,...  47 us
    pallas_call x1, Pallas kernels, project(): pl.pallas_call(project_kernel, out_shape=(jax.ShapeDtypeStruct((2, 512, 1...  30.9 us
    pallas_call x1, Pallas kernels, output(): pl.pallas_call(output_kernel, out_shape=jax.ShapeDtypeStruct((64, 4096),...  24.7 us
    unnamed x17, local copies, waits for them, and re-layouts  7.15 us

profile of v2, /device:TPU:1, one launch (start us, length us, event | category | flops | bytes accessed | tf_op | source)
XLA Modules:
  0.0 110.1 jit_solution(3374151137061628410)
XLA Ops:
  0.0 0.0 copy-start.1
  0.0 1.6 %copy.13.w4 = bf16[4096,64]{1,0:T(8,128)(2,1)S(1)} copy(bf16[4096,64]{0,1:T(8,128)(2,1)} %param.17) | data formatting | bytes 1048576 | tf_op args[5]
  1.6 1.5 %copy.14.w5 = bf16[4096,64]{1,0:T(8,128)(2,1)S(1)} copy(bf16[4096,64]{0,1:T(8,128)(2,1)} %param.18) | data formatting | bytes 1048576 | tf_op args[6]
  3.1 0.0 copy-done.1
  3.1 0.0 copy-start.5
  3.1 0.0 copy-start.6
  3.1 0.0 copy-start.4
  3.2 30.9 %project.1 = (bf16[2,512,128]{2,1,0:T(8,128)(2,1)S(1)}, bf16[2,2,512,128]{3,2,1,0:T(8,128)(2,1)S(1)}, bf16[512,256]{1,0:T(8,128)(2,1)S(1)}, bf16[512,128]{1,0:T(8,128)(2,1)S(1)}) custom-call(bf16[64,4096]{1,0:T(8,128)(2,1)S(1)} %copy-done.1, bf16[4096,256]{1,0:T(8,128)(2,1)} %w0.1, bf16[4096,256]{1,0:T(8,128)(2,1)} %w1.1, bf16[4096,256]{1,0:T(8,128)(2,1)} %w2.1, ...), custom_call_target="tpu_custom_call" | custom-call | tf_op jit(solution)/shard_map/project/pallas_call | solution.py:803
  34.1 0.0 copy-start.2
  34.1 0.7 copy-done.2
  34.8 0.0 copy-done.5
  34.8 0.1 copy.15.gain_in
  34.9 0.0 copy-done.6
  34.9 0.1 broadcast_in_dim.4.lam_in
  35.0 0.0 copy-done.4
  35.0 0.0 copy-start.3
  35.0 1.0 copy-done.3
  35.9 47.0 %attention.1 = (bf16[2,512,128]{2,1,0:T(8,128)(2,1)S(1)}, bf16[512,256]{1,0:T(8,128)(2,1)S(1)}) custom-call(bf16[2,512,128]{2,1,0:T(8,128)(2,1)S(1)} %get-tuple-element.11.q_in, bf16[2,2,512,128]{3,2,1,0:T(8,128)(2,1)S(1)} %get-tuple-element.12.kv_in, bf16[512,256]{1,0:T(8,128)(2,1)S(1)} %copy-done.3, bf16[512,128]{1,0:T(8,128)(2,1)S(1)} %get-tuple-element.14.bkv_in, ...), custom_call_target="tpu_custom_call" | custom-call | tf_op jit(solution)/shard_map/attention/pallas_call | solution.py:489
  83.0 0.0 copy-start
  83.0 1.6 %copy-done = bf16[256,4096]{1,0:T(8,128)(2,1)S(1)} copy-done((bf16[256,4096]{1,0:T(8,128)(2,1)S(1)}, bf16[256,4096]{1,0:T(8,128)(2,1)}, u32[]{:S(2)}) %copy-start) | copy-done | bytes 2097176
  84.6 24.7 %output.1 = bf16[64,4096]{1,0:T(8,128)(2,1)S(1)} custom-call(bf16[2,512,128]{2,1,0:T(8,128)(2,1)S(1)} %get-tuple-element.15.a_in, bf16[512,256]{1,0:T(8,128)(2,1)S(1)} %get-tuple-element.16.b_in, bf16[256,4096]{1,0:T(8,128)(2,1)S(1)} %copy-done, bf16[256,4096]{1,0:T(8,128)(2,1)} %bw_in.1), custom_call_target="tpu_custom_call" | custom-call | tf_op jit(solution)/shard_map/output/pallas_call | solution.py:637
  109.3 0.8 copy.17
Async XLA Ops:
  0.0 3.1 %copy-start.1 = (bf16[64,4096]{1,0:T(8,128)(2,1)S(1)}, bf16[64,4096]{1,0:T(8,128)(2,1)}, u32[]{:S(2)}) copy-start(bf16[64,4096]{1,0:T(8,128)(2,1)} %x_in.1) | copy-start | bytes 1572868
  3.1 31.7 %copy-start.5 = (f32[128]{0:T(128)S(1)}, f32[128]{0:T(128)}, u32[]{:S(2)}) copy-start(f32[128]{0:T(128)} %param.20) | copy-start | bytes 1540
  3.1 31.8 %copy-start.6 = (f32[2]{0:T(128)S(1)}, f32[2]{0:T(128)}, u32[]{:S(2)}) copy-start(f32[2]{0:T(128)} %param.19) | copy-start | bytes 28
  3.1 31.8 %copy-start.4 = (f32[4]{0:T(128)S(1)}, f32[4]{0:T(128)}, u32[]{:S(2)}) copy-start(f32[4]{0:T(128)} %sink_in.1) | copy-start | bytes 52
  34.1 0.7 copy-start.2
  35.0 1.0 copy-start.3
  83.0 1.6 %copy-start = (bf16[256,4096]{1,0:T(8,128)(2,1)S(1)}, bf16[256,4096]{1,0:T(8,128)(2,1)}, u32[]{:S(2)}) copy-start(bf16[256,4096]{1,0:T(8,128)(2,1)} %aw_in.1) | copy-start | bytes 6291460

commit v3 on v1

v3 whole, which is shorter than its diff:
```python
import functools

import jax
import jax.numpy as jnp
from jax import lax
from jax.experimental import pallas as pl
from jax.experimental.pallas import tpu as pltpu
from jax.sharding import PartitionSpec as P

HEAD_DIM = 64
VALUE_DIM = 128
WINDOW = 128

norm_eps = 0.0001
head_scale = 0.8
mask_fill = -1e30

MESH = pl.DeviceIdType.MESH
NT = (((1,), (1,)), ((), ()))
LOG2E = 1.4426950408889634
VMEM = pltpu.VMEM
F32 = jnp.float32
BF16 = jnp.bfloat16


def remote(src, dst, send_sem, recv_sem, row, col):
    return pltpu.make_async_remote_copy(
        src_ref=src,
        dst_ref=dst,
        send_sem=send_sem,
        recv_sem=recv_sem,
        device_id=(row, col),
        device_id_type=MESH,
    )


def soft_chunk(items, score, lookup, mx, ls, acc):
    def weights(i, pieces):
        before = mx[i]
        top = before
        for piece in pieces:
            top = jnp.maximum(top, jnp.max(piece, axis=0, keepdims=True))
        shrink = jnp.exp2(before - top)
        mx[i] = top
        return shrink, [jnp.exp2(piece - top).astype(BF16) for piece in pieces]

    def collect(i, shrink, pieces):
        got = jnp.dot(lookup, jnp.concatenate(pieces, axis=0), preferred_element_type=F32)
        acc[i] = acc[i] * shrink + got[:VALUE_DIM]
        ls[i] = ls[i] * shrink + got[VALUE_DIM : VALUE_DIM + 1]

    now = score(items[0])
    held = None
    for at, i in enumerate(items):
        later = score(items[at + 1]) if at + 1 < len(items) else None
        current = weights(i, now)
        if held is not None:
            collect(items[at - 1], *held)
        held, now = current, later
    collect(items[-1], *held)


NC = 8
CW = 512
GROUPS = 4


def layer_kernel(
    x_in, wq_in, wk_in, wv_in, wbq_in, wbk_in, wbv_in, lam_in, gain_in, sink_in, aw_in, bw_in,
    out,
    rows, wq, wk, wv, wbq, wbkv, q_own, kv_own, bq_own,
    kv, q_raw, q_mul, near, lam, acc, mx, ls, stage, back, b_heads,
    weights, part, crossed, chip, far_l, far_r, got_l, got_r, relayed,
    pw_s, os, orr, xs, xr_s, xds, xdr,
    a2a_s, a2a_r, zs, zr, rs, rr, ds, dr, q_s, q_r, small_s, small_r, ret_s, ret_r,
    w_s, cr_s, cr_r, fs, fr, gs, gr,
):
    s, t = lax.axis_index("sp"), lax.axis_index("tp")
    z, y = s // 4, s % 4
    x, c = t // 2, t % 2
    xr, xl, xf = (x + 1) % 4, (x + 3) % 4, (x + 2) % 4
    other, right, left = 2 * x + 1 - c, 2 * xr + c, 2 * xl + c
    beyond = 2 * xf + c
    up, down = (z + 1) % 4, (z + 3) % 4
    far = (z + 2) % 4
    mate = 3 - z
    side = z + 1 - 2 * (z % 2)
    quarter = 2 * c + z // 2
    lane = lax.broadcasted_iota(jnp.int32, (1, 128), 1)

    loads = [
        pltpu.make_async_copy(wk_in, wk, pw_s.at[0]),
        pltpu.make_async_copy(wv_in, wv, pw_s.at[1]),
        pltpu.make_async_copy(wq_in, wq, pw_s.at[2]),
        pltpu.make_async_copy(wbq_in, wbq, pw_s.at[3]),
        pltpu.make_async_copy(wbk_in, wbkv.at[pl.ds(0, 64)], pw_s.at[4]),
        pltpu.make_async_copy(wbv_in, wbkv.at[pl.ds(64, 64)], pw_s.at[5]),
    ]
    for load in loads:
        load.start()

    def fetch(n, which):
        columns = pl.ds(pl.multiple_of(n * CW, CW), CW)
        source = aw_in if which == 0 else bw_in
        return pltpu.make_async_copy(
            source.at[:, columns], weights.at[n, pl.ds(256 * which, 256)], w_s.at[n, which]
        )

    for n in range(NC):
        fetch(n, 0).start()
        fetch(n, 1).start()

    barrier = pltpu.get_barrier_semaphore()

    def greet(row, col):
        pl.semaphore_signal(barrier, inc=1, device_id=(row, col), device_id_type=MESH)

    for j in range(4):
        for core in range(2):
            if j == 0:
                @pl.when(core != c)
                def _(core=core):
                    greet(4 * z + y, 2 * x + core)
            else:
                greet(4 * z + (y + j) % 4, 2 * x + core)
            greet(4 * mate + (y + j) % 4, 2 * x + core)
    greet(4 * side + y, t)
    greet(s, right)
    greet(s, left)
    rim_up = (y == 3) & (z % 2 == 0)
    rim_down = (y == 0) & (z % 2 == 1)

    @pl.when(rim_up)
    def _():
        greet(s + 1, t)

    @pl.when(rim_down)
    def _():
        greet(s - 1, t)

    pl.semaphore_wait(barrier, 18 + jnp.where(rim_up | rim_down, 1, 0))

    halves = (pl.ds(0, 2048), pl.ds(2048, 2048))
    every = pl.ds(0, 16)

    def mine16(g):
        return pl.ds(pl.multiple_of(16 * g, 16), 16)

    def own_send(g, way, which):
        return remote(
            x_in.at[mine16(g), halves[which]], rows.at[g, t, every, halves[which]],
            os.at[g, way, which], orr.at[g, way, which], s, right if way == 0 else left,
        )

    def own_wait(g, way, which):
        spot = rows.at[g, left if way == 0 else right, every, halves[which]]
        return remote(
            spot, spot, os.at[g, way, which], orr.at[g, way, which],
            s, right if way == 0 else left,
        )

    def xrelay_send(g, way):
        spot = rows.at[g, left if way == 0 else right, every, halves[way]]
        return remote(
            spot, spot, xs.at[g, way], xr_s.at[g, way], s, right if way == 0 else left
        )

    def xrelay_wait(g, way):
        spot = rows.at[g, beyond, every, halves[way]]
        return remote(
            spot, spot, xs.at[g, way], xr_s.at[g, way], s, right if way == 0 else left
        )

    def own_cross(g):
        return remote(x_in.at[mine16(g)], rows.at[g, t], xds.at[g, x], xdr.at[g, x], s, other)

    def xcross(g, where):
        spot = rows.at[g, 2 * where + c]
        return remote(spot, spot, xds.at[g, where], xdr.at[g, where], s, other)

    def xcross_wait(g, where):
        spot = rows.at[g, 2 * where + 1 - c]
        return remote(spot, spot, xds.at[g, where], xdr.at[g, where], s, other)

    def own_start(g):
        own_send(g, 0, 0).start()
        own_send(g, 1, 1).start()
        own_send(g, 0, 1).start()
        own_send(g, 1, 0).start()
        own_cross(g).start()

    def kv_send(g, head, part_of):
        return remote(
            kv_own.at[head, part_of, g], kv.at[part_of, z, g, y],
            a2a_s.at[g, head, part_of], a2a_r.at[g, y],
            4 * z + 2 * c + head, 2 * x + part_of,
        )

    def kv_local(head, part_of):
        return (2 * c + head == y) & (part_of == c)

    def a2a_wait(g, row):
        spot = kv.at[c, z, g, row]
        return remote(spot, spot, a2a_s.at[0, 0, 0], a2a_r.at[g, row], s, other)

    def z_send(g, way):
        spot = kv.at[c, z, g]
        return remote(spot, spot, zs.at[g, way], zr.at[g, way], 4 * (up, down)[way] + y, t)

    def z_wait(g, way):
        spot = kv.at[c, (down, up)[way], g]
        return remote(spot, spot, zs.at[g, way], zr.at[g, way], 4 * (up, down)[way] + y, t)

    def relay_send(g, way):
        spot = kv.at[c, (down, up)[way], g, pl.ds(2 * way, 2)]
        return remote(spot, spot, rs.at[g, way], rr.at[g, way], 4 * (up, down)[way] + y, t)

    def relay_wait(g, way):
        spot = kv.at[c, far, g, pl.ds(2 * way, 2)]
        return remote(spot, spot, rs.at[g, way], rr.at[g, way], 4 * (up, down)[way] + y, t)

    def cross_send(level, g):
        spot = kv.at[c, level, g]
        return remote(spot, spot, ds.at[level, g], dr.at[level, g], s, other)

    def cross_wait(level, g):
        spot = kv.at[1 - c, level, g]
        return remote(spot, spot, ds.at[level, g], dr.at[level, g], s, other)

    def spread(g):
        for j in range(4):
            row = (y + j) % 4
            if j == 0:
                @pl.when(y // 2 != c)
                def _():
                    a2a_wait(g, y).wait_recv()
            else:
                a2a_wait(g, row).wait_recv()
        z_send(g, 0).start()
        z_send(g, 1).start()
        cross_send(z, g).start()

    def zrelay(g):
        z_wait(g, 0).wait_recv()
        relay_send(g, 0).start()
        cross_send(down, g).start()
        z_wait(g, 1).wait_recv()
        relay_send(g, 1).start()
        cross_send(up, g).start()

    def zfar(g):
        relay_wait(g, 0).wait_recv()
        relay_wait(g, 1).wait_recv()
        cross_send(far, g).start()

    own_start(0)
    own_start(1)
    lam_send = remote(lam_in, lam.at[c], small_s.at[0], small_r.at[0], s, other)
    lam_send.start()
    for g in range(GROUPS):
        rows[g, t] = x_in[16 * g : 16 * (g + 1)]
    lam[c] = lam_in[...]
    acc[...] = jnp.zeros_like(acc)
    ls[...] = jnp.zeros_like(ls)
    mx[...] = jnp.full_like(mx, mask_fill)

    @pl.when(s == 0)
    def _():
        near[pl.ds(0, 128)] = jnp.zeros((128, 128), BF16)

    def gather(g, carry):
        own_wait(g, 0, 0).wait_recv()
        xrelay_send(g, 0).start()
        own_wait(g, 1, 1).wait_recv()
        xrelay_send(g, 1).start()

        @pl.when(g < GROUPS - 2)
        def _():
            own_start(g + 2)

        own_wait(g, 0, 1).wait_recv()
        xcross(g, xl).start()
        own_wait(g, 1, 0).wait_recv()
        xcross(g, xr).start()

        @pl.when(g >= 1)
        def _():
            spread(g - 1)

        @pl.when(g >= 2)
        def _():
            zrelay(g - 2)

        xrelay_wait(g, 0).wait_recv()
        xrelay_wait(g, 1).wait_recv()
        xcross(g, xf).start()

        @pl.when(g == 0)
        def _():
            for load in loads[:2]:
                load.wait()

        for where in (x, xl, xr, xf):
            xcross_wait(g, where).wait_recv()
        block = rows[g].reshape(128, 4096)
        keys = jnp.dot(block, wk[...], preferred_element_type=F32)
        values = jnp.dot(block, wv[...], preferred_element_type=F32)
        for head in range(2):
            lanes = slice(128 * head, 128 * (head + 1))
            kv_own[head, 0, g] = keys[:, lanes].astype(BF16)
            kv_own[head, 1, g] = jnp.transpose(values[:, lanes]).astype(BF16)

            @pl.when(2 * c + head == y)
            def _(head=head):
                kv[c, z, g, y] = kv_own[head, c, g]

            for part_of in range(2):
                @pl.when(~kv_local(head, part_of))
                def _(head=head, part_of=part_of):
                    kv_send(g, head, part_of).start()

        @pl.when(g == 0)
        def _():
            for load in loads[2:]:
                load.wait()

        queries = jnp.dot(block, wq[...], preferred_element_type=F32).astype(BF16)
        b_queries = jnp.dot(block, wbq[...], preferred_element_type=F32).astype(BF16)
        b_pair = lax.dot_general(block, wbkv[...], NT, preferred_element_type=F32).astype(BF16)
        for d in range(8):
            spot = pl.ds(pl.multiple_of(64 * d + 16 * g, 16), 16)
            take = slice(16 * d, 16 * (d + 1))
            q_own[0, spot] = queries[take, :128]
            q_own[1, spot] = queries[take, 128:]
            bq_own[spot] = b_queries[take]
            near[pl.ds(pl.multiple_of(128 + 64 * d + 16 * g, 16), 16)] = b_pair[take]
        return carry

    lax.fori_loop(0, GROUPS, gather, 0)

    def q_send(head, k, core):
        goal = z if k == 0 else mate
        return remote(
            q_own.at[head, pl.ds(128 * (2 * core + goal // 2), 128)], q_raw.at[z // 2, y],
            q_s.at[head, k, core], q_r.at[z // 2, y],
            4 * goal + 2 * c + head, 2 * x + core,
        )

    def q_local(head, k, core):
        return (2 * c + head == y) & (core == c) & (k == 0)

    for head in range(2):
        for k in range(2):
            for core in range(2):
                @pl.when(~q_local(head, k, core))
                def _(head=head, k=k, core=core):
                    q_send(head, k, core).start()

        @pl.when(2 * c + head == y)
        def _(head=head):
            q_raw[z // 2, y] = q_own[head, pl.ds(128 * quarter, 128)]

    rim_send = remote(
        near.at[pl.ds(512, 128)], near.at[pl.ds(0, 128)], small_s.at[1], small_r.at[1],
        jnp.minimum(s + 1, 15), t,
    )

    @pl.when(s < 15)
    def _():
        rim_send.start()

    spread(3)
    zrelay(2)
    zfar(0)
    zfar(1)

    @pl.when(s > 0)
    def _():
        rim_send.wait_recv()

    def windowed(block, carry):
        start = pl.multiple_of(block * 128, 128)
        span = near[pl.ds(start, 256)]
        span32 = span.astype(F32)
        turned = jnp.concatenate([span32[:, HEAD_DIM:], span32[:, :HEAD_DIM]], axis=1)
        keys = jnp.where(lane < HEAD_DIM, span32, turned).astype(BF16)
        values = jnp.transpose(span32)[HEAD_DIM:].astype(BF16)
        parts = []
        sinks = []
        for j in range(4):
            own = bq_own[pl.ds(start, 128), 128 * (j // 2) : 128 * (j // 2 + 1)]
            mine = (lane >= HEAD_DIM) if j % 2 else (lane < HEAD_DIM)
            parts.append(jnp.where(mine, own.astype(F32), 0.0).astype(BF16))
            sinks.append(jnp.full((1, 128), sink_in[j] * LOG2E, F32))
        queries = jnp.concatenate(parts, axis=0)
        sink = jnp.concatenate(sinks, axis=1)
        scores = lax.dot_general(keys, queries, NT, preferred_element_type=F32)
        scores = scores * (LOG2E * HEAD_DIM ** (-0.5))
        key_at = lax.broadcasted_iota(jnp.int32, (256, 512), 0)
        query_at = lax.broadcasted_iota(jnp.int32, (256, 512), 1) % 128
        first = jnp.where((s == 0) & (block == 0), 128, 0)
        allowed = (key_at > query_at) & (key_at <= query_at + WINDOW) & (key_at >= first)
        scores = jnp.where(allowed, scores, mask_fill)
        top = jnp.maximum(jnp.max(scores, axis=0, keepdims=True), sink)
        weights = jnp.exp2(scores - top)
        total = jnp.sum(weights, axis=0, keepdims=True) + jnp.exp2(sink - top)
        found = jnp.dot(values, weights.astype(BF16), preferred_element_type=F32) / total
        tall = jnp.concatenate([found[:, 128 * j : 128 * (j + 1)] for j in range(4)], axis=0)
        b_heads[pl.ds(start, 128)] = jnp.transpose(tall).astype(BF16)
        return carry

    lax.fori_loop(0, 4, windowed, 0)

    for pair in range(2):
        for row in range(4):
            @pl.when(~((pair == z // 2) & (row == y) & (y // 2 == c)))
            def _(pair=pair, row=row):
                remote(
                    q_raw.at[pair, row], q_raw.at[pair, row], q_s.at[0, 0, 0],
                    q_r.at[pair, row], s, other,
                ).wait_recv()

    for pair in range(2):
        for row in range(4):
            wide = q_raw[pair, row].astype(F32) * (LOG2E * HEAD_DIM ** (-0.5))
            high = wide.astype(BF16).astype(F32)
            low = wide - high
            for m in range(2):
                mine = (lane >= HEAD_DIM) if m else (lane < HEAD_DIM)
                i = pair * 4 + (row // 2) * 2 + m
                span = slice(128 * (row % 2), 128 * (row % 2) + 128)
                q_mul[i, span, 0:128] = jnp.where(mine, high, 0.0).astype(BF16)
                q_mul[i, span, 128:256] = jnp.where(mine, low, 0.0).astype(BF16)

    def unit(level, pair):
        keys = kv[0, level, pl.ds(2 * pair, 2)].reshape(1024, 128)
        held = kv[1, level, pl.ds(2 * pair, 2)].reshape(1024, 128)
        lookup = jnp.concatenate([held[128 * k : 128 * (k + 1)] for k in range(8)], axis=1)
        lookup = jnp.concatenate([lookup, jnp.ones((16, 1024), BF16)], axis=0)
        return jnp.concatenate([keys, keys], axis=1), lookup

    def small_unit(level, pair, two):
        rows_of = (pl.ds(2 * pair, 2), pl.ds(2 * two, 2))
        keys = kv[0, level, rows_of[0], rows_of[1]].reshape(512, 128)
        held = kv[1, level, rows_of[0], rows_of[1]].reshape(512, 128)
        lookup = jnp.concatenate([held[128 * k : 128 * (k + 1)] for k in range(4)], axis=1)
        lookup = jnp.concatenate([lookup, jnp.ones((16, 512), BF16)], axis=0)
        return jnp.concatenate([keys, keys], axis=1), lookup

    key_at = lax.broadcasted_iota(jnp.int32, (256, 256), 0)
    query_at = lax.broadcasted_iota(jnp.int32, (256, 256), 1)
    apart = 512 * (key_at // 128) + 64 * ((key_at % 128) // 16) + key_at % 16
    apart = apart - (query_at % 128) - 512 * (query_at // 128)

    def attend(level, pair, sel):
        mark = jnp.where(sel == 0, jnp.minimum(z, mate), jnp.maximum(z, mate))

        @pl.when(level < mark)
        def _():
            keys, lookup = unit(level, pair)

            def score(i):
                return [
                    lax.dot_general(
                        keys[256 * k : 256 * (k + 1)], q_mul[i], NT, preferred_element_type=F32
                    )
                    for k in range(4)
                ]

            soft_chunk([sel * 4 + k for k in range(4)], score, lookup, mx, ls, acc)

        @pl.when(level == mark)
        def _():
            def group(at, carry):
                g = jnp.minimum(at, 1)
                two = at // 2
                keys, lookup = small_unit(level, pair, two)
                base = 1024 * (g - two) + 128 * quarter - 32 * pair

                def score(i):
                    return [
                        jnp.where(
                            apart <= base - 16 * k,
                            lax.dot_general(
                                keys[256 * k : 256 * (k + 1)], q_mul[i], NT,
                                preferred_element_type=F32,
                            ),
                            mask_fill,
                        )
                        for k in range(2)
                    ]

                first = sel * 4 + g * 2
                soft_chunk([first, first + 1], score, lookup, mx, ls, acc)
                return carry

            lax.fori_loop(0, 3, group, 0)

    def step(it, carry):
        @pl.when(it == 2)
        def _():
            zfar(2)

        @pl.when(it == 3)
        def _():
            zrelay(3)

        @pl.when(it == 6)
        def _():
            zfar(3)

        level = jnp.where(
            (it == 0) | (it == 3), z,
            jnp.where((it == 1) | (it == 5), down, jnp.where((it == 2) | (it == 6), up, far)),
        )
        pair = jnp.where((it == 3) | (it >= 5), 1, 0)
        cross_wait(level, 2 * pair).wait_recv()
        cross_wait(level, 2 * pair + 1).wait_recv()

        def one(sel, inner):
            attend(level, pair, sel)
            return inner

        lax.fori_loop(0, 2, one, 0)
        return carry

    lax.fori_loop(0, 8, step, 0)

    lam_send.wait_recv()
    mixing = lam[y // 2, y % 2, 0:1, :]
    gain = gain_in[...] * head_scale

    def ret_send(pair, row):
        goal = jnp.minimum(z, mate) if pair == 0 else jnp.maximum(z, mate)
        return remote(
            stage.at[pair, row], back.at[y % 2, pl.ds(128 * quarter, 128)],
            ret_s.at[pair, row], ret_r.at[y % 2, quarter],
            4 * goal + row, 2 * x + y // 2,
        )

    def ret_local(pair, row):
        return (pair == z // 2) & (row == y) & (y // 2 == c)

    for pair in range(2):
        for g in range(2):
            i = pair * 4 + g * 2
            first_mean = acc[i] / ls[i]
            second_mean = acc[i + 1] / ls[i + 1]
            gap = first_mean - mixing * second_mean
            square = jnp.mean(gap * gap, axis=0, keepdims=True)
            done = gap * lax.rsqrt(square + norm_eps) * gain
            tall = jnp.transpose(done).astype(BF16)
            for k in range(2):
                row = 2 * g + k
                stage[pair, row] = tall[128 * k : 128 * (k + 1)]

                @pl.when(~ret_local(pair, row))
                def _(pair=pair, row=row):
                    ret_send(pair, row).start()

                @pl.when(ret_local(pair, row))
                def _(pair=pair, row=row):
                    back[y % 2, pl.ds(128 * quarter, 128)] = stage[pair, row]

    for head in range(2):
        for k in range(4):
            mine = (2 * c + head == y) & (k == quarter)

            @pl.when(~mine)
            def _(head=head, k=k):
                spot = back.at[head, pl.ds(128 * k, 128)]
                remote(spot, spot, ret_s.at[0, 0], ret_r.at[head, k], s, other).wait_recv()

    heads = jnp.concatenate([back[0], back[1], b_heads[...]], axis=1)
    first, second = pl.ds(0, 32), pl.ds(32, 32)

    def cross(n):
        return remote(part.at[n, 1 - c], crossed.at[n], cr_s.at[n], cr_r.at[n], s, other)

    def far_send(n, way):
        rows = first if way == 0 else second
        return remote(
            chip.at[n, xf, rows], (far_l if way == 0 else far_r).at[n],
            fs.at[n, way], fr.at[n, way], s, right if way == 0 else left,
        )

    def near_send(n, way):
        rows = second if way == 0 else first
        return remote(
            chip.at[n, xr if way == 0 else xl, rows], (got_l if way == 0 else got_r).at[n, rows],
            gs.at[n, way, 0], gr.at[n, way, 0], s, right if way == 0 else left,
        )

    def sum_send(n, way):
        rows = first if way == 0 else second
        return remote(
            relayed.at[n, way], (got_l if way == 0 else got_r).at[n, rows],
            gs.at[n, way, 1], gr.at[n, way, 1], s, right if way == 0 else left,
        )

    def multiply(n):
        fetch(n, 0).wait()
        fetch(n, 1).wait()
        partial = jnp.dot(heads, weights[n], preferred_element_type=F32).astype(BF16)
        for col in range(8):
            part[n, col % 2, col // 2] = partial[64 * col : 64 * (col + 1)]
        cross(n).start()

    def join(n):
        cross(n).wait_recv()
        chip[n] = (part[n, c].astype(F32) + crossed[n].astype(F32)).astype(BF16)
        far_send(n, 0).start()
        far_send(n, 1).start()
        near_send(n, 0).start()
        near_send(n, 1).start()

    def pass_on(n, carry):
        far_send(n, 0).wait_recv()
        relayed[n, 0] = (chip[n, xr, first].astype(F32) + far_l[n].astype(F32)).astype(BF16)
        sum_send(n, 0).start()
        far_send(n, 1).wait_recv()
        relayed[n, 1] = (chip[n, xl, second].astype(F32) + far_r[n].astype(F32)).astype(BF16)
        sum_send(n, 1).start()
        return carry

    multiply(0)

    def run(n, carry):
        multiply(n)
        join(n - 1)
        return carry

    lax.fori_loop(1, NC, run, 0)
    join(NC - 1)
    lax.fori_loop(0, NC, pass_on, 0)

    for n in range(NC):
        for way in range(2):
            near_send(n, way).wait_recv()
            sum_send(n, way).wait_recv()
        total = chip[n, x].astype(F32) + got_l[n].astype(F32) + got_r[n].astype(F32)
        out[:, n * CW : (n + 1) * CW] = total.astype(BF16)

    def drain(n, carry):
        cross(n).wait_send()
        for way in range(2):
            far_send(n, way).wait_send()
            near_send(n, way).wait_send()
            sum_send(n, way).wait_send()
        return carry

    lax.fori_loop(0, NC, drain, 0)

    for g in range(GROUPS):
        for head in range(2):
            for part_of in range(2):
                @pl.when(~kv_local(head, part_of))
                def _(g=g, head=head, part_of=part_of):
                    kv_send(g, head, part_of).wait_send()
    for head in range(2):
        for k in range(2):
            for core in range(2):
                @pl.when(~q_local(head, k, core))
                def _(head=head, k=k, core=core):
                    q_send(head, k, core).wait_send()
    lam_send.wait_send()

    @pl.when(s < 15)
    def _():
        rim_send.wait_send()

    def drain_rows(g, carry):
        for way in range(2):
            own_send(g, way, 0).wait_send()
            own_send(g, way, 1).wait_send()
            xrelay_send(g, way).wait_send()
            z_send(g, way).wait_send()
            relay_send(g, way).wait_send()
        own_cross(g).wait_send()
        for where in (xl, xr, xf):
            xcross(g, where).wait_send()
        for level in range(4):
            cross_send(level, g).wait_send()
        return carry

    lax.fori_loop(0, GROUPS, drain_rows, 0)
    for pair in range(2):
        for row in range(4):
            @pl.when(~ret_local(pair, row))
            def _(pair=pair, row=row):
                ret_send(pair, row).wait_send()


def layer(*operands):
    vmem = pl.BlockSpec(memory_space=VMEM)
    hbm = pl.BlockSpec(memory_space=pl.ANY)
    dma = pltpu.SemaphoreType.DMA
    return pl.pallas_call(
        layer_kernel,
        out_shape=jax.ShapeDtypeStruct((64, 4096), BF16),
        in_specs=[vmem] + [hbm] * 6 + [vmem, vmem, pl.BlockSpec(memory_space=pltpu.SMEM)] + [hbm] * 2,
        out_specs=vmem,
        scratch_shapes=[
            VMEM((4, 8, 16, 4096), BF16),
            VMEM((4096, 256), BF16), VMEM((4096, 256), BF16),
            VMEM((4096, 256), BF16), VMEM((4096, 256), BF16), VMEM((128, 4096), BF16),
            VMEM((2, 512, 128), BF16), VMEM((2, 2, 4, 128, 128), BF16), VMEM((512, 256), BF16),
            VMEM((2, 4, 4, 4, 128, 128), BF16),
            VMEM((2, 4, 128, 128), BF16),
            VMEM((8, 256, 256), BF16),
            VMEM((640, 128), BF16),
            VMEM((2, 2, 8, 256), F32),
            VMEM((8, 128, 256), F32),
            VMEM((8, 1, 256), F32),
            VMEM((8, 1, 256), F32),
            VMEM((2, 4, 128, 128), BF16),
            VMEM((2, 512, 128), BF16),
            VMEM((512, 256), BF16),
            VMEM((NC, 512, CW), BF16),
            VMEM((NC, 2, 4, 64, CW), BF16),
            VMEM((NC, 4, 64, CW), BF16),
            VMEM((NC, 4, 64, CW), BF16),
            VMEM((NC, 32, CW), BF16),
            VMEM((NC, 32, CW), BF16),
            VMEM((NC, 64, CW), BF16),
            VMEM((NC, 64, CW), BF16),
            VMEM((NC, 2, 32, CW), BF16),
            dma((6,)), dma((4, 2, 2)), dma((4, 2, 2)), dma((4, 2)), dma((4, 2)),
            dma((4, 4)), dma((4, 4)),
            dma((4, 2, 2)), dma((4, 4)),
            dma((4, 2)), dma((4, 2)),
            dma((4, 2)), dma((4, 2)),
            dma((4, 4)), dma((4, 4)),
            dma((2, 2, 2)), dma((2, 4)),
            dma((2,)), dma((2,)),
            dma((2, 4)), dma((2, 4)),
            dma((NC, 2)), dma((NC,)), dma((NC,)),
            dma((NC, 2)), dma((NC, 2)), dma((NC, 2, 2)), dma((NC, 2, 2)),
        ],
        compiler_params=pltpu.CompilerParams(
            collective_id=0, has_side_effects=True, vmem_limit_bytes=58 * 2**20
        ),
        name="layer",
    )(*operands)


def shards(
    inputs,
    a_query_w,
    a_key_w,
    a_value_w,
    b_query_w,
    b_key_w,
    b_value_w,
    head_lambda,
    head_gain,
    sink_logit,
    a_out_w,
    b_out_w,
):
    lam = jnp.broadcast_to(head_lambda[:, None, None], (2, 8, 256))
    return layer(
        inputs, a_query_w, a_key_w, a_value_w, b_query_w, b_key_w.T, b_value_w.T,
        lam, head_gain[:, None], sink_logit, a_out_w, b_out_w,
    )


def solution(mesh):
    return jax.shard_map(
        shards,
        mesh=mesh,
        in_specs=(
            P(("sp", "tp"), None),
            P(None, "tp"),
            P(None, "tp"),
            P(None, "tp"),
            P(None, "tp"),
            P(None, "tp"),
            P(None, "tp"),
            P("tp"),
            P(),
            P("tp"),
            P("tp", None),
            P("tp", None),
        ),
        out_specs=P(("sp", "tp"), None),
        check_vma=False,
    )
```

time: 163 us -> 106 us (0.65); the launches traced: 161 us -> 106 us
  waiting for transfers between devices: 71.6 us -> 0 us
  Pallas kernels: 44.7 us -> 102 us
  matrix products: 28.4 us -> 0 us
  between operations: 13.5 us -> 0.01 us
  local copies, waits for them, and re-layouts: 2.04 us -> 4.58 us
    pallas_call x1, Pallas kernels: 44.7 us -> 102 us  [layer(): pl.pallas_call(layer_kernel, out_shape=jax.ShapeDtypeStruct((64, 4096), B...]
    all_gather x1 -> x0, waiting for transfers between devices: 36.6 us -> none  [shards(): rows = lax.all_gather(inputs, 'tp', axis=0, tiled=True)]
    reduce_scatter x1 -> x0, waiting for transfers between devices: 34.3 us -> none  [shards(): lax.psum_scatter((jnp.einsum('hqe,hen->qn', a_heads, a_weight, preferred_...]
    dot_general x8 -> x0, matrix products: 28.4 us -> none  [the longest x6 23.8 us: project(): return jnp.dot(rows, matrix, preferred_element_type=F32).astype(BF16)]
  transfers between devices with their start and end apart: 2 -> 0, of which waited for: 2 -> 0; matrix products, arithmetic and copies ran while one was open for 0% -> 0% of each run, Pallas kernels for 0% -> 0%
where the time goes in v3:
time: 106 us
  Pallas kernels  102 us (96%)
  local copies, waits for them, and re-layouts  4.58 us (4%)
    pallas_call x1, Pallas kernels, layer(): pl.pallas_call(layer_kernel, out_shape=jax.ShapeDtypeStruct((64, 4096), B...  102 us

profile of v3, /device:TPU:1, one launch (start us, length us, event | category | flops | bytes accessed | tf_op | source)
XLA Modules:
  0.0 106.3 jit_solution(2483871733805993987)
XLA Ops:
  0.0 1.3 %broadcast_in_dim.4.lam_in = f32[2,8,256]{2,1,0:T(8,128)} broadcast(f32[2]{0:T(128)} %param.19), dimensions={0} | broadcast | bytes 16392 | tf_op jit(solution)/shard_map/broadcast_in_dim | solution.py:761
  1.3 1.4 %copy.13.gain_in = f32[128,1]{1,0:T(8,128)} copy(f32[128,1]{0,1:T(1,128)} %bitcast.5) | data formatting | bytes 1024 | tf_op jit(solution)/shard_map/broadcast_in_dim | solution.py:764
  2.7 101.7 %layer.1 = bf16[64,4096]{1,0:T(8,128)(2,1)} custom-call(bf16[64,4096]{1,0:T(8,128)(2,1)} %x_in.1, bf16[4096,256]{1,0:T(8,128)(2,1)} %wq_in.1, bf16[4096,256]{1,0:T(8,128)(2,1)} %wk_in.1, bf16[4096,256]{1,0:T(8,128)(2,1)} %wv_in.1, bf16[4096,256]{1,0:T(8,128)(2,1)} %wbq_in.1, bf16[64,4096]{1,0:T(8,128)(2,1)} %bitcast.3, bf16[64,4096]{1,0:T(8,128)(2,1)} %bitcast.4, ...), custom_call_target="tpu_custom_call" | custom-call | tf_op jit(solution)/shard_map/layer/pallas_call | solution.py:698
  104.4 1.9 %copy.15 = bf16[64,4096]{1,0:T(8,128)(2,1)} copy(bf16[64,4096]{1,0:T(8,128)(2,1)} %layer.1) | data formatting | bytes 1048576

commit v4 on v3

--- a/solution.py
+++ b/solution.py
@@ -66,14 +66,14 @@
 
 
 def layer_kernel(
-    x_in, wq_in, wk_in, wv_in, wbq_in, wbk_in, wbv_in, lam_in, gain_in, sink_in, aw_in, bw_in,
+    x_hbm, wq_in, wk_in, wv_in, wbq_in, wbk_in, wbv_in, lam_in, gain_in, sink_in, aw_in, bw_in,
     out,
-    rows, wq, wk, wv, wbq, wbkv, q_own, kv_own, bq_own,
+    x_in, rows, wq, wk, wv, wbq, wbkv, q_own, kv_own, bq_own,
     kv, q_raw, q_mul, near, lam, acc, mx, ls, stage, back, b_heads,
     weights, part, crossed, chip, far_l, far_r, got_l, got_r, relayed,
-    pw_s, os, orr, xs, xr_s, xds, xdr,
+    x_s, pw_s, os, orr, xs, xr_s, xds, xdr,
     a2a_s, a2a_r, zs, zr, rs, rr, ds, dr, q_s, q_r, small_s, small_r, ret_s, ret_r,
-    w_s, cr_s, cr_r, fs, fr, gs, gr,
+    w_s, cr_s, cr_r, fs, fr, gs, ss, gr,
 ):
     s, t = lax.axis_index("sp"), lax.axis_index("tp")
     z, y = s // 4, s % 4
@@ -88,27 +88,24 @@
     quarter = 2 * c + z // 2
     lane = lax.broadcasted_iota(jnp.int32, (1, 128), 1)
 
+    x_load = pltpu.make_async_copy(x_hbm, x_in, x_s)
+    x_load.start()
+    mixed = y // 2 == c
     loads = [
+        pltpu.make_async_copy(wq_in, wq, pw_s.at[2]),
         pltpu.make_async_copy(wk_in, wk, pw_s.at[0]),
         pltpu.make_async_copy(wv_in, wv, pw_s.at[1]),
-        pltpu.make_async_copy(wq_in, wq, pw_s.at[2]),
         pltpu.make_async_copy(wbq_in, wbq, pw_s.at[3]),
         pltpu.make_async_copy(wbk_in, wbkv.at[pl.ds(0, 64)], pw_s.at[4]),
         pltpu.make_async_copy(wbv_in, wbkv.at[pl.ds(64, 64)], pw_s.at[5]),
     ]
-    for load in loads:
-        load.start()
 
     def fetch(n, which):
         columns = pl.ds(pl.multiple_of(n * CW, CW), CW)
         source = aw_in if which == 0 else bw_in
         return pltpu.make_async_copy(
-            source.at[:, columns], weights.at[n, pl.ds(256 * which, 256)], w_s.at[n, which]
-        )
-
-    for n in range(NC):
-        fetch(n, 0).start()
-        fetch(n, 1).start()
+            source.at[:, columns], weights.at[n, pl.ds(256 * which, 256)], w_s
+        )
 
     barrier = pltpu.get_barrier_semaphore()
 
@@ -138,6 +135,9 @@
     def _():
         greet(s - 1, t)
 
+    x_load.wait()
+    for load in loads:
+        load.start()
     pl.semaphore_wait(barrier, 18 + jnp.where(rim_up | rim_down, 1, 0))
 
     halves = (pl.ds(0, 2048), pl.ds(2048, 2048))
@@ -149,38 +149,34 @@
     def own_send(g, way, which):
         return remote(
             x_in.at[mine16(g), halves[which]], rows.at[g, t, every, halves[which]],
-            os.at[g, way, which], orr.at[g, way, which], s, right if way == 0 else left,
+            os, orr.at[g, way, which], s, right if way == 0 else left,
         )
 
     def own_wait(g, way, which):
         spot = rows.at[g, left if way == 0 else right, every, halves[which]]
         return remote(
-            spot, spot, os.at[g, way, which], orr.at[g, way, which],
+            spot, spot, os, orr.at[g, way, which],
             s, right if way == 0 else left,
         )
 
     def xrelay_send(g, way):
         spot = rows.at[g, left if way == 0 else right, every, halves[way]]
-        return remote(
-            spot, spot, xs.at[g, way], xr_s.at[g, way], s, right if way == 0 else left
-        )
-
-    def xrelay_wait(g, way):
-        spot = rows.at[g, beyond, every, halves[way]]
-        return remote(
-            spot, spot, xs.at[g, way], xr_s.at[g, way], s, right if way == 0 else left
-        )
+        return remote(spot, spot, xs, xr_s.at[g], s, right if way == 0 else left)
+
+    def xrelay_wait(g):
+        spot = rows.at[g, beyond]
+        return remote(spot, spot, xs, xr_s.at[g], s, right)
 
     def own_cross(g):
-        return remote(x_in.at[mine16(g)], rows.at[g, t], xds.at[g, x], xdr.at[g, x], s, other)
+        return remote(x_in.at[mine16(g)], rows.at[g, t], xds, xdr.at[g], s, other)
 
     def xcross(g, where):
         spot = rows.at[g, 2 * where + c]
-        return remote(spot, spot, xds.at[g, where], xdr.at[g, where], s, other)
-
-    def xcross_wait(g, where):
-        spot = rows.at[g, 2 * where + 1 - c]
-        return remote(spot, spot, xds.at[g, where], xdr.at[g, where], s, other)
+        return remote(spot, spot, xds, xdr.at[g], s, other)
+
+    def xcross_wait(g):
+        spot = rows.at[g, pl.ds(0, 4)]
+        return remote(spot, spot, xds, xdr.at[g], s, other)
 
     def own_start(g):
         own_send(g, 0, 0).start()
@@ -192,50 +188,50 @@
     def kv_send(g, head, part_of):
         return remote(
             kv_own.at[head, part_of, g], kv.at[part_of, z, g, y],
-            a2a_s.at[g, head, part_of], a2a_r.at[g, y],
+            a2a_s, a2a_r.at[g],
             4 * z + 2 * c + head, 2 * x + part_of,
         )
 
     def kv_local(head, part_of):
         return (2 * c + head == y) & (part_of == c)
 
-    def a2a_wait(g, row):
-        spot = kv.at[c, z, g, row]
-        return remote(spot, spot, a2a_s.at[0, 0, 0], a2a_r.at[g, row], s, other)
+    def a2a_wait(g, count):
+        spot = kv.at[c, z, g, pl.ds(0, count)]
+        return remote(spot, spot, a2a_s, a2a_r.at[g], s, other)
 
     def z_send(g, way):
         spot = kv.at[c, z, g]
-        return remote(spot, spot, zs.at[g, way], zr.at[g, way], 4 * (up, down)[way] + y, t)
+        return remote(spot, spot, zs, zr.at[g, way], 4 * (up, down)[way] + y, t)
 
     def z_wait(g, way):
         spot = kv.at[c, (down, up)[way], g]
-        return remote(spot, spot, zs.at[g, way], zr.at[g, way], 4 * (up, down)[way] + y, t)
+        return remote(spot, spot, zs, zr.at[g, way], 4 * (up, down)[way] + y, t)
 
     def relay_send(g, way):
         spot = kv.at[c, (down, up)[way], g, pl.ds(2 * way, 2)]
-        return remote(spot, spot, rs.at[g, way], rr.at[g, way], 4 * (up, down)[way] + y, t)
-
-    def relay_wait(g, way):
-        spot = kv.at[c, far, g, pl.ds(2 * way, 2)]
-        return remote(spot, spot, rs.at[g, way], rr.at[g, way], 4 * (up, down)[way] + y, t)
+        return remote(spot, spot, rs, rr.at[g], 4 * (up, down)[way] + y, t)
+
+    def relay_wait(g):
+        spot = kv.at[c, far, g]
+        return remote(spot, spot, rs, rr.at[g], 4 * up + y, t)
 
     def cross_send(level, g):
         spot = kv.at[c, level, g]
-        return remote(spot, spot, ds.at[level, g], dr.at[level, g], s, other)
-
-    def cross_wait(level, g):
-        spot = kv.at[1 - c, level, g]
-        return remote(spot, spot, ds.at[level, g], dr.at[level, g], s, other)
+        return remote(spot, spot, ds, dr.at[level, g // 2], s, other)
+
+    def cross_wait(level, pair):
+        spot = kv.at[1 - c, level, pl.ds(2 * pair, 2)]
+        return remote(spot, spot, ds, dr.at[level, pair], s, other)
 
     def spread(g):
-        for j in range(4):
-            row = (y + j) % 4
-            if j == 0:
-                @pl.when(y // 2 != c)
-                def _():
-                    a2a_wait(g, y).wait_recv()
-            else:
-                a2a_wait(g, row).wait_recv()
+        @pl.when(mixed)
+        def _():
+            a2a_wait(g, 3).wait_recv()
+
+        @pl.when(~mixed)
+        def _():
+            a2a_wait(g, 4).wait_recv()
+
         z_send(g, 0).start()
         z_send(g, 1).start()
         cross_send(z, g).start()
@@ -249,17 +245,16 @@
         cross_send(up, g).start()
 
     def zfar(g):
-        relay_wait(g, 0).wait_recv()
-        relay_wait(g, 1).wait_recv()
+        relay_wait(g).wait_recv()
         cross_send(far, g).start()
 
     own_start(0)
     own_start(1)
-    lam_send = remote(lam_in, lam.at[c], small_s.at[0], small_r.at[0], s, other)
-    lam_send.start()
+    lam_send = remote(lam.at[c], lam.at[c], small_s.at[0], small_r.at[0], s, other)
     for g in range(GROUPS):
         rows[g, t] = x_in[16 * g : 16 * (g + 1)]
-    lam[c] = lam_in[...]
+    for head in range(2):
+        lam[c, head] = jnp.full((8, 256), lam_in[head], F32)
     acc[...] = jnp.zeros_like(acc)
     ls[...] = jnp.zeros_like(ls)
     mx[...] = jnp.full_like(mx, mask_fill)
@@ -268,7 +263,7 @@
     def _():
         near[pl.ds(0, 128)] = jnp.zeros((128, 128), BF16)
 
-    def gather(g, carry):
+    def near_rows(g):
         own_wait(g, 0, 0).wait_recv()
         xrelay_send(g, 0).start()
         own_wait(g, 1, 1).wait_recv()
@@ -283,26 +278,31 @@
         own_wait(g, 1, 0).wait_recv()
         xcross(g, xr).start()
 
-        @pl.when(g >= 1)
-        def _():
-            spread(g - 1)
+    near_rows(0)
+
+    def gather(g, carry):
+        @pl.when(g < GROUPS - 1)
+        def _():
+            near_rows(g + 1)
+
+        xrelay_wait(g).wait_recv()
+        xcross(g, xf).start()
 
         @pl.when(g >= 2)
         def _():
-            zrelay(g - 2)
-
-        xrelay_wait(g, 0).wait_recv()
-        xrelay_wait(g, 1).wait_recv()
-        xcross(g, xf).start()
+            spread(g - 2)
 
         @pl.when(g == 0)
         def _():
-            for load in loads[:2]:
+            for load in loads[:3]:
                 load.wait()
 
-        for where in (x, xl, xr, xf):
-            xcross_wait(g, where).wait_recv()
+        xcross_wait(g).wait_recv()
         block = rows[g].reshape(128, 4096)
+        queries = jnp.dot(block, wq[...], preferred_element_type=F32).astype(BF16)
+        q_own[0, g] = queries[:, :128]
+        q_own[1, g] = queries[:, 128:]
+        send_queries(g)
         keys = jnp.dot(block, wk[...], preferred_element_type=F32)
         values = jnp.dot(block, wv[...], preferred_element_type=F32)
         for head in range(2):
@@ -321,44 +321,54 @@
 
         @pl.when(g == 0)
         def _():
-            for load in loads[2:]:
+            for load in loads[3:]:
                 load.wait()
-
-        queries = jnp.dot(block, wq[...], preferred_element_type=F32).astype(BF16)
+            for n in range(NC):
+                fetch(n, 0).start()
+                fetch(n, 1).start()
+
+        @pl.when(g == GROUPS - 1)
+        def _():
+            spread(2)
+
         b_queries = jnp.dot(block, wbq[...], preferred_element_type=F32).astype(BF16)
         b_pair = lax.dot_general(block, wbkv[...], NT, preferred_element_type=F32).astype(BF16)
         for d in range(8):
             spot = pl.ds(pl.multiple_of(64 * d + 16 * g, 16), 16)
             take = slice(16 * d, 16 * (d + 1))
-            q_own[0, spot] = queries[take, :128]
-            q_own[1, spot] = queries[take, 128:]
             bq_own[spot] = b_queries[take]
             near[pl.ds(pl.multiple_of(128 + 64 * d + 16 * g, 16), 16)] = b_pair[take]
         return carry
 
-    lax.fori_loop(0, GROUPS, gather, 0)
-
-    def q_send(head, k, core):
+    def q_send(g, head, k, core):
         goal = z if k == 0 else mate
         return remote(
-            q_own.at[head, pl.ds(128 * (2 * core + goal // 2), 128)], q_raw.at[z // 2, y],
-            q_s.at[head, k, core], q_r.at[z // 2, y],
+            q_own.at[head, g, pl.ds(32 * (2 * core + goal // 2), 32)],
+            q_raw.at[4 * (z // 2) + y, g], q_s, q_r,
             4 * goal + 2 * c + head, 2 * x + core,
         )
 
     def q_local(head, k, core):
         return (2 * c + head == y) & (core == c) & (k == 0)
 
-    for head in range(2):
-        for k in range(2):
-            for core in range(2):
-                @pl.when(~q_local(head, k, core))
-                def _(head=head, k=k, core=core):
-                    q_send(head, k, core).start()
-
-        @pl.when(2 * c + head == y)
-        def _(head=head):
-            q_raw[z // 2, y] = q_own[head, pl.ds(128 * quarter, 128)]
+    def send_queries(g):
+        for head in range(2):
+            for k in range(2):
+                for core in range(2):
+                    @pl.when(~q_local(head, k, core))
+                    def _(head=head, k=k, core=core):
+                        q_send(g, head, k, core).start()
+
+            @pl.when(2 * c + head == y)
+            def _(head=head):
+                q_raw[4 * (z // 2) + y, g] = q_own[head, g, pl.ds(32 * quarter, 32)]
+
+    def q_all(count):
+        spot = q_raw.at[pl.ds(0, count)]
+        return remote(spot, spot, q_s, q_r, s, other)
+
+    lam_send.start()
+    lax.fori_loop(0, GROUPS, gather, 0)
 
     rim_send = remote(
         near.at[pl.ds(512, 128)], near.at[pl.ds(0, 128)], small_s.at[1], small_r.at[1],
@@ -369,14 +379,9 @@
     def _():
         rim_send.start()
 
-    spread(3)
-    zrelay(2)
-    zfar(0)
-    zfar(1)
-
-    @pl.when(s > 0)
-    def _():
-        rim_send.wait_recv()
+    zrelay(0)
+    zrelay(1)
+
 
     def windowed(block, carry):
         start = pl.multiple_of(block * 128, 128)
@@ -409,20 +414,24 @@
         b_heads[pl.ds(start, 128)] = jnp.transpose(tall).astype(BF16)
         return carry
 
-    lax.fori_loop(0, 4, windowed, 0)
+    lax.fori_loop(1, 4, windowed, 0)
+
+    spread(3)
+    @pl.when(mixed)
+    def _():
+        q_all(7).wait_recv()
+
+    @pl.when(~mixed)
+    def _():
+        q_all(8).wait_recv()
 
     for pair in range(2):
         for row in range(4):
-            @pl.when(~((pair == z // 2) & (row == y) & (y // 2 == c)))
-            def _(pair=pair, row=row):
-                remote(
-                    q_raw.at[pair, row], q_raw.at[pair, row], q_s.at[0, 0, 0],
-                    q_r.at[pair, row], s, other,
-                ).wait_recv()
-
-    for pair in range(2):
-        for row in range(4):
-            wide = q_raw[pair, row].astype(F32) * (LOG2E * HEAD_DIM ** (-0.5))
+            raw = q_raw[4 * pair + row].astype(F32)
+            raw = jnp.concatenate(
+                [raw[g, 16 * d : 16 * (d + 1)] for d in range(2) for g in range(4)], axis=0
+            )
+            wide = raw * (LOG2E * HEAD_DIM ** (-0.5))
             high = wide.astype(BF16).astype(F32)
             low = wide - high
             for m in range(2):
@@ -497,25 +506,38 @@
             lax.fori_loop(0, 3, group, 0)
 
     def step(it, carry):
+        @pl.when(it == 1)
+        def _():
+            zfar(0)
+
         @pl.when(it == 2)
         def _():
+            zfar(1)
+            zrelay(2)
+
+        @pl.when(it == 3)
+        def _():
+            @pl.when(s > 0)
+            def _():
+                rim_send.wait_recv()
+
+            windowed(0, 0)
+
+        @pl.when(it == 4)
+        def _():
+            zrelay(3)
             zfar(2)
 
-        @pl.when(it == 3)
-        def _():
-            zrelay(3)
-
         @pl.when(it == 6)
         def _():
             zfar(3)
 
+        turn = it % 4
         level = jnp.where(
-            (it == 0) | (it == 3), z,
-            jnp.where((it == 1) | (it == 5), down, jnp.where((it == 2) | (it == 6), up, far)),
-        )
-        pair = jnp.where((it == 3) | (it >= 5), 1, 0)
-        cross_wait(level, 2 * pair).wait_recv()
-        cross_wait(level, 2 * pair + 1).wait_recv()
+            turn == 0, z, jnp.where(turn == 1, down, jnp.where(turn == 2, up, far))
+        )
+        pair = it // 4
+        cross_wait(level, pair).wait_recv()
 
         def one(sel, inner):
             attend(level, pair, sel)
@@ -533,8 +555,7 @@
     def ret_send(pair, row):
         goal = jnp.minimum(z, mate) if pair == 0 else jnp.maximum(z, mate)
         return remote(
-            stage.at[pair, row], back.at[y % 2, pl.ds(128 * quarter, 128)],
-            ret_s.at[pair, row], ret_r.at[y % 2, quarter],
+            stage.at[4 * pair + row], back.at[4 * (y % 2) + quarter], ret_s, ret_r,
             4 * goal + row, 2 * x + y // 2,
         )
 
@@ -548,11 +569,11 @@
             second_mean = acc[i + 1] / ls[i + 1]
             gap = first_mean - mixing * second_mean
             square = jnp.mean(gap * gap, axis=0, keepdims=True)
-            done = gap * lax.rsqrt(square + norm_eps) * gain
-            tall = jnp.transpose(done).astype(BF16)
+            done = gap * lax.rsqrt(square + norm_eps)
+            tall = (jnp.transpose(done) * gain).astype(BF16)
             for k in range(2):
                 row = 2 * g + k
-                stage[pair, row] = tall[128 * k : 128 * (k + 1)]
+                stage[4 * pair + row] = tall[128 * k : 128 * (k + 1)]
 
                 @pl.when(~ret_local(pair, row))
                 def _(pair=pair, row=row):
@@ -560,47 +581,50 @@
 
                 @pl.when(ret_local(pair, row))
                 def _(pair=pair, row=row):
-                    back[y % 2, pl.ds(128 * quarter, 128)] = stage[pair, row]
-
-    for head in range(2):
-        for k in range(4):
-            mine = (2 * c + head == y) & (k == quarter)
-
-            @pl.when(~mine)
-            def _(head=head, k=k):
-                spot = back.at[head, pl.ds(128 * k, 128)]
-                remote(spot, spot, ret_s.at[0, 0], ret_r.at[head, k], s, other).wait_recv()
-
-    heads = jnp.concatenate([back[0], back[1], b_heads[...]], axis=1)
+                    back[4 * (y % 2) + quarter] = stage[4 * pair + row]
+
+    def ret_all(count):
+        spot = back.at[pl.ds(0, count)]
+        return remote(spot, spot, ret_s, ret_r, s, other)
+
+    @pl.when(mixed)
+    def _():
+        ret_all(7).wait_recv()
+
+    @pl.when(~mixed)
+    def _():
+        ret_all(8).wait_recv()
+
+    heads = jnp.concatenate(
+        [back[0:4].reshape(512, 128), back[4:8].reshape(512, 128), b_heads[...]], axis=1
+    )
     first, second = pl.ds(0, 32), pl.ds(32, 32)
 
     def cross(n):
-        return remote(part.at[n, 1 - c], crossed.at[n], cr_s.at[n], cr_r.at[n], s, other)
+        return remote(part.at[n, 1 - c], crossed.at[n], cr_s, cr_r.at[n], s, other)
 
     def far_send(n, way):
         rows = first if way == 0 else second
         return remote(
             chip.at[n, xf, rows], (far_l if way == 0 else far_r).at[n],
-            fs.at[n, way], fr.at[n, way], s, right if way == 0 else left,
+            fs, fr.at[n], s, right if way == 0 else left,
         )
 
     def near_send(n, way):
         rows = second if way == 0 else first
         return remote(
             chip.at[n, xr if way == 0 else xl, rows], (got_l if way == 0 else got_r).at[n, rows],
-            gs.at[n, way, 0], gr.at[n, way, 0], s, right if way == 0 else left,
+            gs, gr.at[n], s, right if way == 0 else left,
         )
 
     def sum_send(n, way):
         rows = first if way == 0 else second
         return remote(
             relayed.at[n, way], (got_l if way == 0 else got_r).at[n, rows],
-            gs.at[n, way, 1], gr.at[n, way, 1], s, right if way == 0 else left,
+            ss, gr.at[n], s, right if way == 0 else left,
         )
 
     def multiply(n):
-        fetch(n, 0).wait()
-        fetch(n, 1).wait()
         partial = jnp.dot(heads, weights[n], preferred_element_type=F32).astype(BF16)
         for col in range(8):
             part[n, col % 2, col // 2] = partial[64 * col : 64 * (col + 1)]
@@ -615,14 +639,14 @@
         near_send(n, 1).start()
 
     def pass_on(n, carry):
-        far_send(n, 0).wait_recv()
+        remote(relayed.at[n], relayed.at[n], fs, fr.at[n], s, right).wait_recv()
         relayed[n, 0] = (chip[n, xr, first].astype(F32) + far_l[n].astype(F32)).astype(BF16)
         sum_send(n, 0).start()
-        far_send(n, 1).wait_recv()
         relayed[n, 1] = (chip[n, xl, second].astype(F32) + far_r[n].astype(F32)).astype(BF16)
         sum_send(n, 1).start()
         return carry
 
+    remote(weights, weights, gs, w_s, s, other).wait_recv()
     multiply(0)
 
     def run(n, carry):
@@ -632,89 +656,72 @@
 
     lax.fori_loop(1, NC, run, 0)
     join(NC - 1)
+    def drained(spot, sem):
+        remote(spot, spot, sem, q_r, s, other).wait_send()
+
+    drained(rows.at[0], os)
+    drained(x_in, xs)
+    drained(rows.at[pl.ds(0, 2)], xds)
+    drained(kv.at[0, pl.ds(0, 2)], zs)
+    drained(kv.at[0, 0], rs)
+    drained(kv.at[0], ds)
+    lam_send.wait_send()
+
+    @pl.when(s < 15)
+    def _():
+        rim_send.wait_send()
+
+    @pl.when(mixed)
+    def _():
+        drained(kv.at[0, 0, pl.ds(0, 3)], a2a_s)
+        q_all(7).wait_send()
+        ret_all(7).wait_send()
+
+    @pl.when(~mixed)
+    def _():
+        drained(kv.at[0, 0], a2a_s)
+        q_all(8).wait_send()
+        ret_all(8).wait_send()
+
     lax.fori_loop(0, NC, pass_on, 0)
 
+    drained(crossed, cr_s)
+    drained(relayed, fs)
+    drained(relayed, gs)
     for n in range(NC):
-        for way in range(2):
-            near_send(n, way).wait_recv()
-            sum_send(n, way).wait_recv()
+        spot = chip.at[n, pl.ds(0, 2)]
+        remote(spot, spot, ss, gr.at[n], s, other).wait_recv()
         total = chip[n, x].astype(F32) + got_l[n].astype(F32) + got_r[n].astype(F32)
         out[:, n * CW : (n + 1) * CW] = total.astype(BF16)
-
-    def drain(n, carry):
-        cross(n).wait_send()
-        for way in range(2):
-            far_send(n, way).wait_send()
-            near_send(n, way).wait_send()
-            sum_send(n, way).wait_send()
-        return carry
-
-    lax.fori_loop(0, NC, drain, 0)
-
-    for g in range(GROUPS):
-        for head in range(2):
-            for part_of in range(2):
-                @pl.when(~kv_local(head, part_of))
-                def _(g=g, head=head, part_of=part_of):
-                    kv_send(g, head, part_of).wait_send()
-    for head in range(2):
-        for k in range(2):
-            for core in range(2):
-                @pl.when(~q_local(head, k, core))
-                def _(head=head, k=k, core=core):
-                    q_send(head, k, core).wait_send()
-    lam_send.wait_send()
-
-    @pl.when(s < 15)
-    def _():
-        rim_send.wait_send()
-
-    def drain_rows(g, carry):
-        for way in range(2):
-            own_send(g, way, 0).wait_send()
-            own_send(g, way, 1).wait_send()
-            xrelay_send(g, way).wait_send()
-            z_send(g, way).wait_send()
-            relay_send(g, way).wait_send()
-        own_cross(g).wait_send()
-        for where in (xl, xr, xf):
-            xcross(g, where).wait_send()
-        for level in range(4):
-            cross_send(level, g).wait_send()
-        return carry
-
-    lax.fori_loop(0, GROUPS, drain_rows, 0)
-    for pair in range(2):
-        for row in range(4):
-            @pl.when(~ret_local(pair, row))
-            def _(pair=pair, row=row):
-                ret_send(pair, row).wait_send()
+    drained(relayed, ss)
 
 
 def layer(*operands):
     vmem = pl.BlockSpec(memory_space=VMEM)
-    hbm = pl.BlockSpec(memory_space=pl.ANY)
+    hbm = pl.BlockSpec(memory_space=pltpu.HBM)
+    smem = pl.BlockSpec(memory_space=pltpu.SMEM)
     dma = pltpu.SemaphoreType.DMA
     return pl.pallas_call(
         layer_kernel,
         out_shape=jax.ShapeDtypeStruct((64, 4096), BF16),
-        in_specs=[vmem] + [hbm] * 6 + [vmem, vmem, pl.BlockSpec(memory_space=pltpu.SMEM)] + [hbm] * 2,
+        in_specs=[hbm] * 7 + [smem, vmem, smem] + [hbm] * 2,
         out_specs=vmem,
         scratch_shapes=[
+            VMEM((64, 4096), BF16),
             VMEM((4, 8, 16, 4096), BF16),
             VMEM((4096, 256), BF16), VMEM((4096, 256), BF16),
             VMEM((4096, 256), BF16), VMEM((4096, 256), BF16), VMEM((128, 4096), BF16),
-            VMEM((2, 512, 128), BF16), VMEM((2, 2, 4, 128, 128), BF16), VMEM((512, 256), BF16),
+            VMEM((2, 4, 128, 128), BF16), VMEM((2, 2, 4, 128, 128), BF16), VMEM((512, 256), BF16),
             VMEM((2, 4, 4, 4, 128, 128), BF16),
-            VMEM((2, 4, 128, 128), BF16),
+            VMEM((8, 4, 32, 128), BF16),
             VMEM((8, 256, 256), BF16),
             VMEM((640, 128), BF16),
             VMEM((2, 2, 8, 256), F32),
             VMEM((8, 128, 256), F32),
             VMEM((8, 1, 256), F32),
             VMEM((8, 1, 256), F32),
-            VMEM((2, 4, 128, 128), BF16),
-            VMEM((2, 512, 128), BF16),
+            VMEM((8, 128, 128), BF16),
+            VMEM((8, 128, 128), BF16),
             VMEM((512, 256), BF16),
             VMEM((NC, 512, CW), BF16),
             VMEM((NC, 2, 4, 64, CW), BF16),
@@ -725,20 +732,13 @@
             VMEM((NC, 64, CW), BF16),
             VMEM((NC, 64, CW), BF16),
             VMEM((NC, 2, 32, CW), BF16),
-            dma((6,)), dma((4, 2, 2)), dma((4, 2, 2)), dma((4, 2)), dma((4, 2)),
-            dma((4, 4)), dma((4, 4)),
-            dma((4, 2, 2)), dma((4, 4)),
-            dma((4, 2)), dma((4, 2)),
-            dma((4, 2)), dma((4, 2)),
-            dma((4, 4)), dma((4, 4)),
-            dma((2, 2, 2)), dma((2, 4)),
-            dma((2,)), dma((2,)),
-            dma((2, 4)), dma((2, 4)),
-            dma((NC, 2)), dma((NC,)), dma((NC,)),
-            dma((NC, 2)), dma((NC, 2)), dma((NC, 2, 2)), dma((NC, 2, 2)),
+            dma, dma((6,)), dma, dma((4, 2, 2)), dma, dma((4,)), dma, dma((4,)),
+            dma, dma((4,)), dma, dma((4, 2)), dma, dma((4,)), dma, dma((4, 2)),
+            dma, dma, dma((2,)), dma((2,)), dma, dma,
+            dma, dma, dma((NC,)), dma, dma((NC,)), dma, dma, dma((NC,)),
         ],
         compiler_params=pltpu.CompilerParams(
-            collective_id=0, has_side_effects=True, vmem_limit_bytes=58 * 2**20
+            collective_id=0, has_side_effects=True, vmem_limit_bytes=56 * 2**20
         ),
         name="layer",
     )(*operands)
@@ -758,10 +758,9 @@
     a_out_w,
     b_out_w,
 ):
-    lam = jnp.broadcast_to(head_lambda[:, None, None], (2, 8, 256))
     return layer(
         inputs, a_query_w, a_key_w, a_value_w, b_query_w, b_key_w.T, b_value_w.T,
-        lam, head_gain[:, None], sink_logit, a_out_w, b_out_w,
+        head_lambda, head_gain[None], sink_logit, a_out_w, b_out_w,
     )
 
 

time: 106 us -> 88.8 us (0.84)
  Pallas kernels: 102 us -> 86.7 us
  local copies, waits for them, and re-layouts: 4.58 us -> 1.87 us
    pallas_call x1, Pallas kernels: 102 us -> 86.7 us  [layer(): pl.pallas_call(layer_kernel, out_shape=jax.ShapeDtypeStruct((64, 4096), B...]
    broadcast_in_dim x2 -> x0, local copies, waits for them, and re-layouts: 2.71 us -> none  [the longest x1 1.39 us: shards(): head_gain[:, None]]
where the time goes in v4:
time: 88.8 us; the launch traced here: 88.6 us
  Pallas kernels  86.7 us (98%)
  local copies, waits for them, and re-layouts  1.87 us (2%)
    pallas_call x1, Pallas kernels, layer(): pl.pallas_call(layer_kernel, out_shape=jax.ShapeDtypeStruct((64, 4096), B...  86.7 us
    unnamed x1, local copies, waits for them, and re-layouts  1.87 us

profile of v4, /device:TPU:1, one launch (start us, length us, event | category | flops | bytes accessed | tf_op | source)
XLA Modules:
  0.0 88.6 jit_solution(14790351833452284920)
XLA Ops:
  0.0 86.7 %layer.1 = bf16[64,4096]{1,0:T(8,128)(2,1)} custom-call(bf16[64,4096]{1,0:T(8,128)(2,1)} %x_hbm.1, bf16[4096,256]{1,0:T(8,128)(2,1)} %wq_in.1, bf16[4096,256]{1,0:T(8,128)(2,1)} %wk_in.1, bf16[4096,256]{1,0:T(8,128)(2,1)} %wv_in.1, bf16[4096,256]{1,0:T(8,128)(2,1)} %wbq_in.1, bf16[64,4096]{1,0:T(8,128)(2,1)} %bitcast.3, bf16[64,4096]{1,0:T(8,128)(2,1)} %bitcast.4, ...), custom_call_target="tpu_custom_call" | custom-call | tf_op jit(solution)/shard_map/layer/pallas_call | solution.py:704
  86.7 1.9 %copy.14 = bf16[64,4096]{1,0:T(8,128)(2,1)} copy(bf16[64,4096]{1,0:T(8,128)(2,1)} %layer.1) | data formatting | bytes 1048576

commit v5 on v4

--- a/solution.py
+++ b/solution.py
@@ -34,7 +34,7 @@
     )
 
 
-def soft_chunk(items, score, lookup, mx, ls, acc):
+def soft_chunk(items, mx, ls, acc):
     def weights(i, pieces):
         before = mx[i]
         top = before
@@ -44,20 +44,20 @@
         mx[i] = top
         return shrink, [jnp.exp2(piece - top).astype(BF16) for piece in pieces]
 
-    def collect(i, shrink, pieces):
+    def collect(i, lookup, shrink, pieces):
         got = jnp.dot(lookup, jnp.concatenate(pieces, axis=0), preferred_element_type=F32)
         acc[i] = acc[i] * shrink + got[:VALUE_DIM]
         ls[i] = ls[i] * shrink + got[VALUE_DIM : VALUE_DIM + 1]
 
-    now = score(items[0])
+    now = items[0][1]()
     held = None
-    for at, i in enumerate(items):
-        later = score(items[at + 1]) if at + 1 < len(items) else None
-        current = weights(i, now)
+    for at, (i, _, lookup) in enumerate(items):
+        later = items[at + 1][1]() if at + 1 < len(items) else None
+        current = (i, lookup, *weights(i, now))
         if held is not None:
-            collect(items[at - 1], *held)
+            collect(*held)
         held, now = current, later
-    collect(items[-1], *held)
+    collect(*held)
 
 
 NC = 8
@@ -68,10 +68,10 @@
 def layer_kernel(
     x_hbm, wq_in, wk_in, wv_in, wbq_in, wbk_in, wbv_in, lam_in, gain_in, sink_in, aw_in, bw_in,
     out,
-    x_in, rows, wq, wk, wv, wbq, wbkv, q_own, kv_own, bq_own,
+    out_v, x_in, rows, wa, wbq, wbkv, q_own, kv_own, bq_own,
     kv, q_raw, q_mul, near, lam, acc, mx, ls, stage, back, b_heads,
     weights, part, crossed, chip, far_l, far_r, got_l, got_r, relayed,
-    x_s, pw_s, os, orr, xs, xr_s, xds, xdr,
+    out_s, x_s, pw_s, os, orr, xs, xr_s, xds, xdr,
     a2a_s, a2a_r, zs, zr, rs, rr, ds, dr, q_s, q_r, small_s, small_r, ret_s, ret_r,
     w_s, cr_s, cr_r, fs, fr, gs, ss, gr,
 ):
@@ -92,9 +92,9 @@
     x_load.start()
     mixed = y // 2 == c
     loads = [
-        pltpu.make_async_copy(wq_in, wq, pw_s.at[2]),
-        pltpu.make_async_copy(wk_in, wk, pw_s.at[0]),
-        pltpu.make_async_copy(wv_in, wv, pw_s.at[1]),
+        pltpu.make_async_copy(wq_in, wa.at[:, pl.ds(0, 256)], pw_s.at[2]),
+        pltpu.make_async_copy(wk_in, wa.at[:, pl.ds(256, 256)], pw_s.at[0]),
+        pltpu.make_async_copy(wv_in, wa.at[:, pl.ds(512, 256)], pw_s.at[1]),
         pltpu.make_async_copy(wbq_in, wbq, pw_s.at[3]),
         pltpu.make_async_copy(wbk_in, wbkv.at[pl.ds(0, 64)], pw_s.at[4]),
         pltpu.make_async_copy(wbv_in, wbkv.at[pl.ds(64, 64)], pw_s.at[5]),
@@ -269,9 +269,10 @@
         own_wait(g, 1, 1).wait_recv()
         xrelay_send(g, 1).start()
 
-        @pl.when(g < GROUPS - 2)
-        def _():
-            own_start(g + 2)
+        @pl.when(g == 0)
+        def _():
+            own_start(2)
+            own_start(3)
 
         own_wait(g, 0, 1).wait_recv()
         xcross(g, xl).start()
@@ -279,18 +280,39 @@
         xcross(g, xr).start()
 
     near_rows(0)
-
-    def gather(g, carry):
-        @pl.when(g < GROUPS - 1)
-        def _():
-            near_rows(g + 1)
-
+    near_rows(1)
+
+    def far_rows(g):
         xrelay_wait(g).wait_recv()
         xcross(g, xf).start()
 
-        @pl.when(g >= 2)
-        def _():
-            spread(g - 2)
+    def project_b(at, count):
+        block = rows[at : at + count].reshape(128 * count, 4096)
+        b_queries = jnp.dot(block, wbq[...], preferred_element_type=F32).astype(BF16)
+        b_pair = lax.dot_general(block, wbkv[...], NT, preferred_element_type=F32).astype(BF16)
+        for k in range(count):
+            for d in range(8):
+                first_row = 64 * d + 16 * (at + k)
+                take = slice(128 * k + 16 * d, 128 * k + 16 * (d + 1))
+                bq_own[first_row : first_row + 16] = b_queries[take]
+                near[first_row + 128 : first_row + 144] = b_pair[take]
+
+    def gather(g, carry):
+        @pl.when(g == 0)
+        def _():
+            far_rows(0)
+            near_rows(2)
+
+        @pl.when(g == 1)
+        def _():
+            near_rows(3)
+            far_rows(1)
+            far_rows(2)
+            spread(0)
+
+        @pl.when(g == 2)
+        def _():
+            far_rows(3)
 
         @pl.when(g == 0)
         def _():
@@ -299,12 +321,10 @@
 
         xcross_wait(g).wait_recv()
         block = rows[g].reshape(128, 4096)
-        queries = jnp.dot(block, wq[...], preferred_element_type=F32).astype(BF16)
-        q_own[0, g] = queries[:, :128]
-        q_own[1, g] = queries[:, 128:]
-        send_queries(g)
-        keys = jnp.dot(block, wk[...], preferred_element_type=F32)
-        values = jnp.dot(block, wv[...], preferred_element_type=F32)
+        found = jnp.dot(block, wa[...], preferred_element_type=F32)
+        q_own[0, g] = found[:, :128].astype(BF16)
+        q_own[1, g] = found[:, 128:256].astype(BF16)
+        keys, values = found[:, 256:512], found[:, 512:]
         for head in range(2):
             lanes = slice(128 * head, 128 * (head + 1))
             kv_own[head, 0, g] = keys[:, lanes].astype(BF16)
@@ -319,25 +339,17 @@
                 def _(head=head, part_of=part_of):
                     kv_send(g, head, part_of).start()
 
+        send_queries(g)
+
         @pl.when(g == 0)
         def _():
-            for load in loads[3:]:
-                load.wait()
             for n in range(NC):
                 fetch(n, 0).start()
                 fetch(n, 1).start()
-
-        @pl.when(g == GROUPS - 1)
-        def _():
-            spread(2)
-
-        b_queries = jnp.dot(block, wbq[...], preferred_element_type=F32).astype(BF16)
-        b_pair = lax.dot_general(block, wbkv[...], NT, preferred_element_type=F32).astype(BF16)
-        for d in range(8):
-            spot = pl.ds(pl.multiple_of(64 * d + 16 * g, 16), 16)
-            take = slice(16 * d, 16 * (d + 1))
-            bq_own[spot] = b_queries[take]
-            near[pl.ds(pl.multiple_of(128 + 64 * d + 16 * g, 16), 16)] = b_pair[take]
+            for load in loads[3:]:
+                load.wait()
+            project_b(0, 1)
+
         return carry
 
     def q_send(g, head, k, core):
@@ -369,6 +381,11 @@
 
     lam_send.start()
     lax.fori_loop(0, GROUPS, gather, 0)
+    zrelay(0)
+    project_b(1, 1)
+    spread(1)
+    project_b(2, 2)
+    spread(2)
 
     rim_send = remote(
         near.at[pl.ds(512, 128)], near.at[pl.ds(0, 128)], small_s.at[1], small_r.at[1],
@@ -378,10 +395,6 @@
     @pl.when(s < 15)
     def _():
         rim_send.start()
-
-    zrelay(0)
-    zrelay(1)
-
 
     def windowed(block, carry):
         start = pl.multiple_of(block * 128, 128)
@@ -414,9 +427,9 @@
         b_heads[pl.ds(start, 128)] = jnp.transpose(tall).astype(BF16)
         return carry
 
-    lax.fori_loop(1, 4, windowed, 0)
-
+    windowed(1, 0)
     spread(3)
+
     @pl.when(mixed)
     def _():
         q_all(7).wait_recv()
@@ -433,13 +446,13 @@
             )
             wide = raw * (LOG2E * HEAD_DIM ** (-0.5))
             high = wide.astype(BF16).astype(F32)
-            low = wide - high
+            both = jnp.transpose(jnp.concatenate([high, wide - high], axis=1))
+            tall = lax.broadcasted_iota(jnp.int32, (256, 1), 0) % 128
             for m in range(2):
-                mine = (lane >= HEAD_DIM) if m else (lane < HEAD_DIM)
+                mine = (tall >= HEAD_DIM) if m else (tall < HEAD_DIM)
                 i = pair * 4 + (row // 2) * 2 + m
                 span = slice(128 * (row % 2), 128 * (row % 2) + 128)
-                q_mul[i, span, 0:128] = jnp.where(mine, high, 0.0).astype(BF16)
-                q_mul[i, span, 128:256] = jnp.where(mine, low, 0.0).astype(BF16)
+                q_mul[i, :, span] = jnp.where(mine, both, 0.0).astype(BF16)
 
     def unit(level, pair):
         keys = kv[0, level, pl.ds(2 * pair, 2)].reshape(1024, 128)
@@ -464,58 +477,60 @@
     def attend(level, pair, sel):
         mark = jnp.where(sel == 0, jnp.minimum(z, mate), jnp.maximum(z, mate))
 
+        def score(keys, i):
+            return [
+                jnp.dot(keys[256 * k : 256 * (k + 1)], q_mul[i], preferred_element_type=F32)
+                for k in range(2)
+            ]
+
         @pl.when(level < mark)
         def _():
             keys, lookup = unit(level, pair)
-
-            def score(i):
+            items = []
+            for h in range(2):
+                span = slice(512 * h, 512 * (h + 1))
+                for k in range(4):
+                    i = sel * 4 + k
+                    items.append(
+                        (i, functools.partial(score, keys[span], i), lookup[:, span])
+                    )
+            soft_chunk(items, mx, ls, acc)
+
+        @pl.when(level == mark)
+        def _():
+            base = 128 * quarter - 32 * pair
+
+            def hidden(keys, i):
                 return [
-                    lax.dot_general(
-                        keys[256 * k : 256 * (k + 1)], q_mul[i], NT, preferred_element_type=F32
-                    )
-                    for k in range(4)
+                    jnp.where(apart <= base - 16 * k, piece, mask_fill)
+                    for k, piece in enumerate(score(keys, i))
                 ]
 
-            soft_chunk([sel * 4 + k for k in range(4)], score, lookup, mx, ls, acc)
-
-        @pl.when(level == mark)
-        def _():
-            def group(at, carry):
-                g = jnp.minimum(at, 1)
-                two = at // 2
-                keys, lookup = small_unit(level, pair, two)
-                base = 1024 * (g - two) + 128 * quarter - 32 * pair
-
-                def score(i):
-                    return [
-                        jnp.where(
-                            apart <= base - 16 * k,
-                            lax.dot_general(
-                                keys[256 * k : 256 * (k + 1)], q_mul[i], NT,
-                                preferred_element_type=F32,
-                            ),
-                            mask_fill,
-                        )
-                        for k in range(2)
-                    ]
-
-                first = sel * 4 + g * 2
-                soft_chunk([first, first + 1], score, lookup, mx, ls, acc)
-                return carry
-
-            lax.fori_loop(0, 3, group, 0)
+            items = []
+            low = small_unit(level, pair, 0)
+            high = small_unit(level, pair, 1)
+            for g, (keys, lookup), rule in ((0, low, hidden), (1, low, score), (1, high, hidden)):
+                for m in range(2):
+                    i = sel * 4 + g * 2 + m
+                    items.append((i, functools.partial(rule, keys, i), lookup))
+            soft_chunk(items, mx, ls, acc)
 
     def step(it, carry):
         @pl.when(it == 1)
         def _():
+            zrelay(1)
             zfar(0)
 
-        @pl.when(it == 2)
+        @pl.when((it == 2) | (it == 3))
+        def _():
+            windowed(it, 0)
+            zrelay(it)
+
+        @pl.when(it == 3)
         def _():
             zfar(1)
-            zrelay(2)
-
-        @pl.when(it == 3)
+
+        @pl.when(it == 4)
         def _():
             @pl.when(s > 0)
             def _():
@@ -523,20 +538,21 @@
 
             windowed(0, 0)
 
-        @pl.when(it == 4)
-        def _():
-            zrelay(3)
+        @pl.when(it == 5)
+        def _():
             zfar(2)
 
         @pl.when(it == 6)
         def _():
             zfar(3)
 
-        turn = it % 4
         level = jnp.where(
-            turn == 0, z, jnp.where(turn == 1, down, jnp.where(turn == 2, up, far))
-        )
-        pair = it // 4
+            it < 2, z,
+            jnp.where(
+                (it == 2) | (it == 5), down, jnp.where((it == 3) | (it == 6), up, far)
+            ),
+        )
+        pair = jnp.where((it == 1) | (it >= 5), 1, 0)
         cross_wait(level, pair).wait_recv()
 
         def one(sel, inner):
@@ -692,8 +708,10 @@
         spot = chip.at[n, pl.ds(0, 2)]
         remote(spot, spot, ss, gr.at[n], s, other).wait_recv()
         total = chip[n, x].astype(F32) + got_l[n].astype(F32) + got_r[n].astype(F32)
-        out[:, n * CW : (n + 1) * CW] = total.astype(BF16)
+        out_v[n] = total.astype(BF16)
+        pltpu.make_async_copy(out_v.at[n], out.at[:, pl.ds(n * CW, CW)], out_s).start()
     drained(relayed, ss)
+    pltpu.make_async_copy(x_in, out, out_s).wait()
 
 
 def layer(*operands):
@@ -705,12 +723,12 @@
         layer_kernel,
         out_shape=jax.ShapeDtypeStruct((64, 4096), BF16),
         in_specs=[hbm] * 7 + [smem, vmem, smem] + [hbm] * 2,
-        out_specs=vmem,
+        out_specs=hbm,
         scratch_shapes=[
+            VMEM((NC, 64, CW), BF16),
             VMEM((64, 4096), BF16),
             VMEM((4, 8, 16, 4096), BF16),
-            VMEM((4096, 256), BF16), VMEM((4096, 256), BF16),
-            VMEM((4096, 256), BF16), VMEM((4096, 256), BF16), VMEM((128, 4096), BF16),
+            VMEM((4096, 768), BF16), VMEM((4096, 256), BF16), VMEM((128, 4096), BF16),
             VMEM((2, 4, 128, 128), BF16), VMEM((2, 2, 4, 128, 128), BF16), VMEM((512, 256), BF16),
             VMEM((2, 4, 4, 4, 128, 128), BF16),
             VMEM((8, 4, 32, 128), BF16),
@@ -732,7 +750,7 @@
             VMEM((NC, 64, CW), BF16),
             VMEM((NC, 64, CW), BF16),
             VMEM((NC, 2, 32, CW), BF16),
-            dma, dma((6,)), dma, dma((4, 2, 2)), dma, dma((4,)), dma, dma((4,)),
+            dma, dma, dma((6,)), dma, dma((4, 2, 2)), dma, dma((4,)), dma, dma((4,)),
             dma, dma((4,)), dma, dma((4, 2)), dma, dma((4,)), dma, dma((4, 2)),
             dma, dma, dma((2,)), dma((2,)), dma, dma,
             dma, dma, dma((NC,)), dma, dma((NC,)), dma, dma, dma((NC,)),

time: 88.8 us -> 86.9 us (0.979)
  Pallas kernels: 86.7 us -> 84.8 us
    pallas_call x1, Pallas kernels: 86.7 us -> 84.8 us  [layer(): pl.pallas_call(layer_kernel, out_shape=jax.ShapeDtypeStruct((64, 4096), B...]
where the time goes in v5:
time: 86.9 us; the launch traced here: 86.7 us
  Pallas kernels  84.8 us (98%)
  local copies, waits for them, and re-layouts  1.87 us (2%)
    pallas_call x1, Pallas kernels, layer(): pl.pallas_call(layer_kernel, out_shape=jax.ShapeDtypeStruct((64, 4096), B...  84.8 us
    unnamed x1, local copies, waits for them, and re-layouts  1.87 us

profile of v5, /device:TPU:1, one launch (start us, length us, event | category | flops | bytes accessed | tf_op | source)
XLA Modules:
  0.0 86.7 jit_solution(15022022435055601835)
XLA Ops:
  0.0 84.8 %layer.1 = bf16[64,4096]{1,0:T(8,128)(2,1)} custom-call(bf16[64,4096]{1,0:T(8,128)(2,1)} %x_hbm.1, bf16[4096,256]{1,0:T(8,128)(2,1)} %wq_in.1, bf16[4096,256]{1,0:T(8,128)(2,1)} %wk_in.1, bf16[4096,256]{1,0:T(8,128)(2,1)} %wv_in.1, bf16[4096,256]{1,0:T(8,128)(2,1)} %wbq_in.1, bf16[64,4096]{1,0:T(8,128)(2,1)} %bitcast.3, bf16[64,4096]{1,0:T(8,128)(2,1)} %bitcast.4, ...), custom_call_target="tpu_custom_call" | custom-call | tf_op jit(solution)/shard_map/layer/pallas_call | solution.py:722
  84.9 1.9 %copy.14 = bf16[64,4096]{1,0:T(8,128)(2,1)} copy(bf16[64,4096]{1,0:T(8,128)(2,1)} %layer.1) | data formatting | bytes 1048576

commit v6 on v5

--- a/solution.py
+++ b/solution.py
@@ -86,6 +86,7 @@
     mate = 3 - z
     side = z + 1 - 2 * (z % 2)
     quarter = 2 * c + z // 2
+    most = jnp.maximum(z, mate)
     lane = lax.broadcasted_iota(jnp.int32, (1, 128), 1)
 
     x_load = pltpu.make_async_copy(x_hbm, x_in, x_s)
@@ -211,6 +212,10 @@
         spot = kv.at[c, (down, up)[way], g, pl.ds(2 * way, 2)]
         return remote(spot, spot, rs, rr.at[g], 4 * (up, down)[way] + y, t)
 
+    def relay_whole(g):
+        spot = kv.at[c, up, g]
+        return remote(spot, spot, rs, rr.at[g], 4 * down + y, t)
+
     def relay_wait(g):
         spot = kv.at[c, far, g]
         return remote(spot, spot, rs, rr.at[g], 4 * up + y, t)
@@ -233,20 +238,41 @@
             a2a_wait(g, 4).wait_recv()
 
         z_send(g, 0).start()
-        z_send(g, 1).start()
+
+        @pl.when(z < 3)
+        def _():
+            z_send(g, 1).start()
+
         cross_send(z, g).start()
 
     def zrelay(g):
         z_wait(g, 0).wait_recv()
-        relay_send(g, 0).start()
+
+        @pl.when(z >= 2)
+        def _():
+            relay_send(g, 0).start()
+
         cross_send(down, g).start()
-        z_wait(g, 1).wait_recv()
-        relay_send(g, 1).start()
-        cross_send(up, g).start()
+
+        @pl.when(z != 2)
+        def _():
+            z_wait(g, 1).wait_recv()
+
+            @pl.when(z == 3)
+            def _():
+                relay_whole(g).start()
+
+            @pl.when(z < 2)
+            def _():
+                relay_send(g, 1).start()
+
+            cross_send(up, g).start()
 
     def zfar(g):
-        relay_wait(g).wait_recv()
-        cross_send(far, g).start()
+        @pl.when(z != 1)
+        def _():
+            relay_wait(g).wait_recv()
+            cross_send(far, g).start()
 
     own_start(0)
     own_start(1)
@@ -269,10 +295,9 @@
         own_wait(g, 1, 1).wait_recv()
         xrelay_send(g, 1).start()
 
-        @pl.when(g == 0)
-        def _():
-            own_start(2)
-            own_start(3)
+        @pl.when(g < GROUPS - 2)
+        def _():
+            own_start(g + 2)
 
         own_wait(g, 0, 1).wait_recv()
         xcross(g, xl).start()
@@ -305,13 +330,17 @@
 
         @pl.when(g == 1)
         def _():
+            far_rows(1)
+
+        @pl.when(g == 2)
+        def _():
             near_rows(3)
-            far_rows(1)
+            spread(0)
             far_rows(2)
-            spread(0)
-
-        @pl.when(g == 2)
-        def _():
+
+        @pl.when(g == 3)
+        def _():
+            spread(1)
             far_rows(3)
 
         @pl.when(g == 0)
@@ -381,11 +410,10 @@
 
     lam_send.start()
     lax.fori_loop(0, GROUPS, gather, 0)
+    project_b(1, 1)
+    spread(2)
+    project_b(2, 2)
     zrelay(0)
-    project_b(1, 1)
-    spread(1)
-    project_b(2, 2)
-    spread(2)
 
     rim_send = remote(
         near.at[pl.ds(512, 128)], near.at[pl.ds(0, 128)], small_s.at[1], small_r.at[1],
@@ -521,10 +549,12 @@
             zrelay(1)
             zfar(0)
 
-        @pl.when((it == 2) | (it == 3))
-        def _():
-            windowed(it, 0)
-            zrelay(it)
+        @pl.when(it == 2)
+        def _():
+            windowed(2, 0)
+            zrelay(2)
+            windowed(3, 0)
+            zrelay(3)
 
         @pl.when(it == 3)
         def _():
@@ -541,9 +571,6 @@
         @pl.when(it == 5)
         def _():
             zfar(2)
-
-        @pl.when(it == 6)
-        def _():
             zfar(3)
 
         level = jnp.where(
@@ -553,13 +580,16 @@
             ),
         )
         pair = jnp.where((it == 1) | (it >= 5), 1, 0)
-        cross_wait(level, pair).wait_recv()
-
-        def one(sel, inner):
-            attend(level, pair, sel)
-            return inner
-
-        lax.fori_loop(0, 2, one, 0)
+        @pl.when(level <= most)
+        def _():
+            cross_wait(level, pair).wait_recv()
+
+            def one(sel, inner):
+                attend(level, pair, sel)
+                return inner
+
+            lax.fori_loop(0, 2, one, 0)
+
         return carry
 
     lax.fori_loop(0, 8, step, 0)
@@ -678,9 +708,25 @@
     drained(rows.at[0], os)
     drained(x_in, xs)
     drained(rows.at[pl.ds(0, 2)], xds)
-    drained(kv.at[0, pl.ds(0, 2)], zs)
-    drained(kv.at[0, 0], rs)
-    drained(kv.at[0], ds)
+    @pl.when(z == 3)
+    def _():
+        drained(kv.at[0, 0], zs)
+        drained(kv.at[0, 0], rs)
+        drained(kv.at[0, 0, pl.ds(0, 2)], rs)
+
+    @pl.when(z < 3)
+    def _():
+        drained(kv.at[0, pl.ds(0, 2)], zs)
+        drained(kv.at[0, 0, pl.ds(0, 2)], rs)
+
+    @pl.when((z == 0) | (z == 3))
+    def _():
+        drained(kv.at[0], ds)
+
+    @pl.when((z == 1) | (z == 2))
+    def _():
+        drained(kv.at[0, pl.ds(0, 3)], ds)
+
     lam_send.wait_send()
 
     @pl.when(s < 15)

time: 86.9 us -> 85.5 us (0.984)
  Pallas kernels: 84.8 us -> 83.4 us
    pallas_call x1, Pallas kernels: 84.8 us -> 83.4 us  [layer(): pl.pallas_call(layer_kernel, out_shape=jax.ShapeDtypeStruct((64, 4096), B...]
where the time goes in v6:
time: 85.5 us; the launch traced here: 85.3 us
  Pallas kernels  83.4 us (98%)
  local copies, waits for them, and re-layouts  1.87 us (2%)
    pallas_call x1, Pallas kernels, layer(): pl.pallas_call(layer_kernel, out_shape=jax.ShapeDtypeStruct((64, 4096), B...  83.4 us
    unnamed x1, local copies, waits for them, and re-layouts  1.87 us

profile of v6, /device:TPU:1, one launch (start us, length us, event | category | flops | bytes accessed | tf_op | source)
XLA Modules:
  0.0 85.3 jit_solution(5343294821169919346)
XLA Ops:
  0.0 83.4 %layer.1 = bf16[64,4096]{1,0:T(8,128)(2,1)} custom-call(bf16[64,4096]{1,0:T(8,128)(2,1)} %x_hbm.1, bf16[4096,256]{1,0:T(8,128)(2,1)} %wq_in.1, bf16[4096,256]{1,0:T(8,128)(2,1)} %wk_in.1, bf16[4096,256]{1,0:T(8,128)(2,1)} %wv_in.1, bf16[4096,256]{1,0:T(8,128)(2,1)} %wbq_in.1, bf16[64,4096]{1,0:T(8,128)(2,1)} %bitcast.3, bf16[64,4096]{1,0:T(8,128)(2,1)} %bitcast.4, ...), custom_call_target="tpu_custom_call" | custom-call | tf_op jit(solution)/shard_map/layer/pallas_call | solution.py:768
  83.5 1.9 %copy.14 = bf16[64,4096]{1,0:T(8,128)(2,1)} copy(bf16[64,4096]{1,0:T(8,128)(2,1)} %layer.1) | data formatting | bytes 1048576

commit v7 on v6

--- a/solution.py
+++ b/solution.py
@@ -66,12 +66,12 @@
 
 
 def layer_kernel(
-    x_hbm, wq_in, wk_in, wv_in, wbq_in, wbk_in, wbv_in, lam_in, gain_in, sink_in, aw_in, bw_in,
+    x_hbm, wq_in, wk_in, wv_in, wbq_in, wbk_in, wbv_in, few_in, aw_in, bw_in,
     out,
-    out_v, x_in, rows, wa, wbq, wbkv, q_own, kv_own, bq_own,
+    x_in, rows, wa, wbq, wbkv, q_own, kv_own, bq_own,
     kv, q_raw, q_mul, near, lam, acc, mx, ls, stage, back, b_heads,
     weights, part, crossed, chip, far_l, far_r, got_l, got_r, relayed,
-    out_s, x_s, pw_s, os, orr, xs, xr_s, xds, xdr,
+    x_s, pw_s, os, orr, xs, xr_s, xds, xdr,
     a2a_s, a2a_r, zs, zr, rs, rr, ds, dr, q_s, q_r, small_s, small_r, ret_s, ret_r,
     w_s, cr_s, cr_r, fs, fr, gs, ss, gr,
 ):
@@ -280,7 +280,7 @@
     for g in range(GROUPS):
         rows[g, t] = x_in[16 * g : 16 * (g + 1)]
     for head in range(2):
-        lam[c, head] = jnp.full((8, 256), lam_in[head], F32)
+        lam[c, head] = jnp.broadcast_to(few_in[0:1, head : head + 1], (8, 256))
     acc[...] = jnp.zeros_like(acc)
     ls[...] = jnp.zeros_like(ls)
     mx[...] = jnp.full_like(mx, mask_fill)
@@ -437,7 +437,7 @@
             own = bq_own[pl.ds(start, 128), 128 * (j // 2) : 128 * (j // 2 + 1)]
             mine = (lane >= HEAD_DIM) if j % 2 else (lane < HEAD_DIM)
             parts.append(jnp.where(mine, own.astype(F32), 0.0).astype(BF16))
-            sinks.append(jnp.full((1, 128), sink_in[j] * LOG2E, F32))
+            sinks.append(jnp.broadcast_to(few_in[0:1, 2 + j : 3 + j] * LOG2E, (1, 128)))
         queries = jnp.concatenate(parts, axis=0)
         sink = jnp.concatenate(sinks, axis=1)
         scores = lax.dot_general(keys, queries, NT, preferred_element_type=F32)
@@ -596,7 +596,7 @@
 
     lam_send.wait_recv()
     mixing = lam[y // 2, y % 2, 0:1, :]
-    gain = gain_in[...] * head_scale
+    gain = few_in[:, 128:256] * head_scale
 
     def ret_send(pair, row):
         goal = jnp.minimum(z, mate) if pair == 0 else jnp.maximum(z, mate)
@@ -754,24 +754,20 @@
         spot = chip.at[n, pl.ds(0, 2)]
         remote(spot, spot, ss, gr.at[n], s, other).wait_recv()
         total = chip[n, x].astype(F32) + got_l[n].astype(F32) + got_r[n].astype(F32)
-        out_v[n] = total.astype(BF16)
-        pltpu.make_async_copy(out_v.at[n], out.at[:, pl.ds(n * CW, CW)], out_s).start()
+        out[:, n * CW : (n + 1) * CW] = total.astype(BF16)
     drained(relayed, ss)
-    pltpu.make_async_copy(x_in, out, out_s).wait()
 
 
 def layer(*operands):
     vmem = pl.BlockSpec(memory_space=VMEM)
     hbm = pl.BlockSpec(memory_space=pltpu.HBM)
-    smem = pl.BlockSpec(memory_space=pltpu.SMEM)
     dma = pltpu.SemaphoreType.DMA
     return pl.pallas_call(
         layer_kernel,
         out_shape=jax.ShapeDtypeStruct((64, 4096), BF16),
-        in_specs=[hbm] * 7 + [smem, vmem, smem] + [hbm] * 2,
-        out_specs=hbm,
+        in_specs=[hbm] * 7 + [vmem] + [hbm] * 2,
+        out_specs=vmem,
         scratch_shapes=[
-            VMEM((NC, 64, CW), BF16),
             VMEM((64, 4096), BF16),
             VMEM((4, 8, 16, 4096), BF16),
             VMEM((4096, 768), BF16), VMEM((4096, 256), BF16), VMEM((128, 4096), BF16),
@@ -796,13 +792,13 @@
             VMEM((NC, 64, CW), BF16),
             VMEM((NC, 64, CW), BF16),
             VMEM((NC, 2, 32, CW), BF16),
-            dma, dma, dma((6,)), dma, dma((4, 2, 2)), dma, dma((4,)), dma, dma((4,)),
+            dma, dma((6,)), dma, dma((4, 2, 2)), dma, dma((4,)), dma, dma((4,)),
             dma, dma((4,)), dma, dma((4, 2)), dma, dma((4,)), dma, dma((4, 2)),
             dma, dma, dma((2,)), dma((2,)), dma, dma,
             dma, dma, dma((NC,)), dma, dma((NC,)), dma, dma, dma((NC,)),
         ],
         compiler_params=pltpu.CompilerParams(
-            collective_id=0, has_side_effects=True, vmem_limit_bytes=56 * 2**20
+            collective_id=0, has_side_effects=True, vmem_limit_bytes=int(53.2 * 2**20)
         ),
         name="layer",
     )(*operands)
@@ -822,9 +818,10 @@
     a_out_w,
     b_out_w,
 ):
+    few = jnp.concatenate([head_lambda, sink_logit, jnp.zeros((122,), F32), head_gain])[None]
     return layer(
         inputs, a_query_w, a_key_w, a_value_w, b_query_w, b_key_w.T, b_value_w.T,
-        head_lambda, head_gain[None], sink_logit, a_out_w, b_out_w,
+        few, a_out_w, b_out_w,
     )
 
 

time: 85.5 us -> 83.7 us (0.979)
  Pallas kernels: 83.4 us -> 81.9 us
  local copies, waits for them, and re-layouts: 1.87 us -> 0.8 us
    pallas_call x1, Pallas kernels: 83.4 us -> 81.9 us  [layer(): pl.pallas_call(layer_kernel, out_shape=jax.ShapeDtypeStruct((64, 4096), B...]
    unnamed x1, local copies, waits for them, and re-layouts: 1.87 us -> 0.8 us
where the time goes in v7:
time: 83.7 us; the launch traced here: 83.5 us
  Pallas kernels  81.9 us (98%)
    pallas_call x1, Pallas kernels, layer(): pl.pallas_call(layer_kernel, out_shape=jax.ShapeDtypeStruct((64, 4096), B...  81.9 us

profile of v7, /device:TPU:1, one launch (start us, length us, event | category | flops | bytes accessed | tf_op | source)
XLA Modules:
  0.0 83.5 jit_solution(3135101412255378311)
XLA Ops:
  0.0 0.8 pad_maximum_fusion
  0.8 81.9 %layer.1 = bf16[64,4096]{1,0:T(8,128)(2,1)S(1)} custom-call(bf16[64,4096]{1,0:T(8,128)(2,1)} %x_hbm.1, bf16[4096,256]{1,0:T(8,128)(2,1)} %wq_in.1, bf16[4096,256]{1,0:T(8,128)(2,1)} %wk_in.1, bf16[4096,256]{1,0:T(8,128)(2,1)} %wv_in.1, bf16[4096,256]{1,0:T(8,128)(2,1)} %wbq_in.1, bf16[64,4096]{1,0:T(8,128)(2,1)} %bitcast.4, bf16[64,4096]{1,0:T(8,128)(2,1)} %bitcast.5, ...), custom_call_target="tpu_custom_call" | custom-call | tf_op jit(solution)/shard_map/layer/pallas_call | solution.py:765
  82.7 0.8 copy.14
  (1 shorter events, 0.0 us)

commit v8 on v7

--- a/solution.py
+++ b/solution.py
@@ -543,57 +543,6 @@
                     items.append((i, functools.partial(rule, keys, i), lookup))
             soft_chunk(items, mx, ls, acc)
 
-    def step(it, carry):
-        @pl.when(it == 1)
-        def _():
-            zrelay(1)
-            zfar(0)
-
-        @pl.when(it == 2)
-        def _():
-            windowed(2, 0)
-            zrelay(2)
-            windowed(3, 0)
-            zrelay(3)
-
-        @pl.when(it == 3)
-        def _():
-            zfar(1)
-
-        @pl.when(it == 4)
-        def _():
-            @pl.when(s > 0)
-            def _():
-                rim_send.wait_recv()
-
-            windowed(0, 0)
-
-        @pl.when(it == 5)
-        def _():
-            zfar(2)
-            zfar(3)
-
-        level = jnp.where(
-            it < 2, z,
-            jnp.where(
-                (it == 2) | (it == 5), down, jnp.where((it == 3) | (it == 6), up, far)
-            ),
-        )
-        pair = jnp.where((it == 1) | (it >= 5), 1, 0)
-        @pl.when(level <= most)
-        def _():
-            cross_wait(level, pair).wait_recv()
-
-            def one(sel, inner):
-                attend(level, pair, sel)
-                return inner
-
-            lax.fori_loop(0, 2, one, 0)
-
-        return carry
-
-    lax.fori_loop(0, 8, step, 0)
-
     lam_send.wait_recv()
     mixing = lam[y // 2, y % 2, 0:1, :]
     gain = few_in[:, 128:256] * head_scale
@@ -608,7 +557,7 @@
     def ret_local(pair, row):
         return (pair == z // 2) & (row == y) & (y // 2 == c)
 
-    for pair in range(2):
+    def finish(pair):
         for g in range(2):
             i = pair * 4 + g * 2
             first_mean = acc[i] / ls[i]
@@ -628,6 +577,67 @@
                 @pl.when(ret_local(pair, row))
                 def _(pair=pair, row=row):
                     back[4 * (y % 2) + quarter] = stage[4 * pair + row]
+
+    def step(it, carry):
+        @pl.when(it == 1)
+        def _():
+            zrelay(1)
+            zfar(0)
+
+        @pl.when(it == 2)
+        def _():
+            windowed(2, 0)
+            zrelay(2)
+            windowed(3, 0)
+            zrelay(3)
+
+        @pl.when(it == 3)
+        def _():
+            zfar(1)
+
+        @pl.when(it == 4)
+        def _():
+            @pl.when(s > 0)
+            def _():
+                rim_send.wait_recv()
+
+            windowed(0, 0)
+
+        @pl.when(it == 5)
+        def _():
+            zfar(2)
+            zfar(3)
+
+        @pl.when((it == 7) & (z != 2))
+        def _():
+            finish(0)
+
+        level = jnp.where(
+            it < 2, z,
+            jnp.where(
+                (it == 2) | (it == 5), down, jnp.where((it == 3) | (it == 6), up, far)
+            ),
+        )
+        pair = jnp.where((it == 1) | (it >= 5), 1, 0)
+        @pl.when(level <= most)
+        def _():
+            cross_wait(level, pair).wait_recv()
+
+            def one(sel, inner):
+                attend(level, pair, sel)
+                return inner
+
+            lax.fori_loop(0, 2, one, 0)
+
+        return carry
+
+    lax.fori_loop(0, 8, step, 0)
+
+    @pl.when(z == 2)
+    def _():
+        finish(0)
+
+    finish(1)
 
     def ret_all(count):
         spot = back.at[pl.ds(0, count)]

time: 83.7 us -> 82.2 us (0.982)
  Pallas kernels: 81.9 us -> 80.5 us
    pallas_call x1, Pallas kernels: 81.9 us -> 80.5 us  [layer(): pl.pallas_call(layer_kernel, out_shape=jax.ShapeDtypeStruct((64, 4096), B...]
where the time goes in v8:
time: 82.2 us; the launch traced here: 82.1 us
  Pallas kernels  80.5 us (98%)
    pallas_call x1, Pallas kernels, layer(): pl.pallas_call(layer_kernel, out_shape=jax.ShapeDtypeStruct((64, 4096), B...  80.5 us

profile of v8, /device:TPU:1, one launch (start us, length us, event | category | flops | bytes accessed | tf_op | source)
XLA Modules:
  0.0 82.1 jit_solution(10209690390773580382)
XLA Ops:
  0.0 0.8 pad_maximum_fusion
  0.8 80.5 %layer.1 = bf16[64,4096]{1,0:T(8,128)(2,1)S(1)} custom-call(bf16[64,4096]{1,0:T(8,128)(2,1)} %x_hbm.1, bf16[4096,256]{1,0:T(8,128)(2,1)} %wq_in.1, bf16[4096,256]{1,0:T(8,128)(2,1)} %wk_in.1, bf16[4096,256]{1,0:T(8,128)(2,1)} %wv_in.1, bf16[4096,256]{1,0:T(8,128)(2,1)} %wbq_in.1, bf16[64,4096]{1,0:T(8,128)(2,1)} %bitcast.4, bf16[64,4096]{1,0:T(8,128)(2,1)} %bitcast.5, ...), custom_call_target="tpu_custom_call" | custom-call | tf_op jit(solution)/shard_map/layer/pallas_call | solution.py:775
  81.3 0.8 copy.14
  (1 shorter events, 0.0 us)
